TPU v7x, 128 devices: a whole 4x4x4 slice. The times are simulated.
128 devices in a mesh: ep: 32 (over z, y, core), tp: 4 (over x).
Axes of the slice: x: 4, y: 4, z: 4, core: 2. Of those that a mesh axis runs over, the one named last changes fastest.
Arguments:
- queries: bfloat16 [16384, 2048], P('ep', 'tp'), may hold values from -6 to 6
- key_rows: bfloat16 [16384, 2048], P('ep', 'tp'), may hold values from -6 to 6
- value_rows: bfloat16 [16384, 4096], P('ep', 'tp'), may hold values from -6 to 6
- gate_rows: bfloat16 [16384, 4096], P('ep', 'tp'), may hold values from -6 to 6
- log_decay: float32 [16, 16384], P('tp', 'ep'), may hold values from -1 to 0
- head_gain: float32 [4096], P('tp'), may hold values from 0.1 to 1.9
- out_weight: bfloat16 [4096, 4096], P('tp'), may hold values from -0.09375 to 0.09375
- expert_input: bfloat16 [16384, 4096], P('ep'), may hold values from -6 to 6
- input_gain: float32 [4096], replicated, may hold values from 0.1 to 1.9
- route_ids: int32 [16384, 2], P('ep'), may hold values from 0 to 31, as said below
- route_weight: float32 [16384, 2], P('ep'), may hold values from 0.1 to 0.9
- expert_gate: bfloat16 [32, 4096, 1024], P('ep', None, 'tp'), may hold values from -0.09375 to 0.09375
- expert_up: bfloat16 [32, 4096, 1024], P('ep', None, 'tp'), may hold values from -0.09375 to 0.09375
- expert_down: bfloat16 [32, 1024, 4096], P('ep', 'tp'), may hold values from -0.1875 to 0.1875
Outputs:
- mixer_out: bfloat16 [16384, 4096], P(('ep', 'tp'))
- expert_out: bfloat16 [16384, 4096], P('ep', 'tp')
Inputs may be any that keep to these rules, and one draw needn't show every extreme that they name: `route_ids`: each row names two different experts of one group of 8 consecutive experts. On the rows of one device each group is named by exactly 128 rows, experts 2 i and 2 i + 1 together are named exactly 4 * 48 / 3 times, and no expert is named by more than 48 rows; one expert is named by exactly 48 rows of every device.
All inputs are finite; a program needn't handle non-finite values.
Results may differ from a plain program's by a relative error of at most 0.019.
Values may be sent and summed in bfloat16 or wider, within the bound.
A program may use at most 192 MiB of HBM per device.

v0:
```python
import jax
import jax.numpy as jnp
from jax import lax
from jax.sharding import PartitionSpec as P

BLOCK = 512


epsilon = 1e-06
theta_base = 10000.0


def prefix(value, axis, combine, identity):
    length, index = (lax.axis_size(axis), lax.axis_index(axis))
    everything = jax.tree.map(
        lambda part, kind: lax.all_gather(part.astype(kind), axis),
        value,
        (jnp.bfloat16, jnp.bfloat16),
    )
    start = jax.tree.map(
        lambda part, zero: jnp.broadcast_to(jnp.asarray(zero, part.dtype), part.shape),
        value,
        identity,
    )

    def hop(k, before):
        reached = k < index
        new = combine(
            before, jax.tree.map(lambda part, own: part[k].astype(own.dtype), everything, value)
        )
        return jax.tree.map(lambda a, b: jnp.where(reached, a, b), new, before)

    return lax.fori_loop(0, length, hop, start)


def rotate(values, positions):
    half_dim = values.shape[-1] // 2
    frequency = theta_base ** (-jnp.arange(half_dim, dtype=jnp.float32) / half_dim)
    angles = positions.astype(jnp.float32)[:, None, None] * frequency
    cosine = jnp.cos(angles)
    sine_wave = jnp.sin(angles)
    first_half = values[..., :half_dim]
    second = values[..., half_dim:]
    return jnp.concatenate(
        [first_half * cosine - second * sine_wave, second * cosine + first_half * sine_wave],
        axis=-1,
    )


def to_blocks(array, blocks):
    return array.reshape(blocks, array.shape[0] // blocks, array.shape[1], array.shape[2])


def combine_states(earlier, later):
    return (later[1][:, None, None] * earlier[0] + later[0], earlier[1] * later[1])


def retention_rows(queries, key_rows, value_rows, gate_rows, log_decay, head_gain):
    length = queries.shape[0]
    head_count = log_decay.shape[0]
    key_width = queries.shape[1] // head_count
    value_width = value_rows.shape[1] // head_count
    blocks = length // BLOCK
    positions = lax.axis_index("ep") * length + jnp.arange(length, dtype=jnp.int32)
    query_rot = to_blocks(
        rotate(queries.astype(jnp.float32).reshape(length, head_count, key_width), positions),
        blocks,
    )
    key_rot = to_blocks(
        rotate(key_rows.astype(jnp.float32).reshape(length, head_count, key_width), positions)
        * key_width ** (-0.5),
        blocks,
    )
    value_all = to_blocks(
        value_rows.astype(jnp.float32).reshape(length, head_count, value_width), blocks
    )
    running = jnp.cumsum(log_decay.reshape(head_count, blocks, BLOCK), axis=2)
    ending = running[:, :, -1]
    kept = jnp.exp(ending[:, :, None] - running)
    block_states = jnp.einsum("nlhd,hnl,nlhe->nhde", key_rot, kept, value_all)
    block_decay = jnp.exp(ending).T

    def advance(carried, inputs):
        decay_now, state_now = inputs
        return (decay_now[:, None, None] * carried + state_now, carried)

    zeros_state = jnp.zeros((head_count, key_width, value_width), jnp.float32)
    device_state, local_starts = lax.scan(advance, zeros_state, (block_decay, block_states))
    device_decay = jnp.exp(jnp.sum(ending, axis=1))
    incoming, passed_decay = prefix(
        (device_state, device_decay),
        "ep",
        combine_states,
        (zeros_state, jnp.ones((head_count,), jnp.float32)),
    )
    causal = jnp.arange(BLOCK)[:, None] >= jnp.arange(BLOCK)[None, :]
    spread = running[:, :, :, None] - running[:, :, None, :]
    weight_table = jnp.exp(jnp.where(causal, spread, -jnp.inf))
    score_matrix = jnp.einsum("nlhd,nmhd->hnlm", query_rot, key_rot) * weight_table
    inside = jnp.einsum("hnlm,nmhe->nlhe", score_matrix, value_all)
    before = jnp.exp(jnp.cumsum(ending, axis=1) - ending)
    starts = local_starts + before.T[:, :, None, None] * incoming[None]
    outside = jnp.einsum("nlhd,hnl,nhde->nlhe", query_rot, jnp.exp(running), starts)
    mixed = (inside + outside).reshape(length, head_count, value_width)
    centered = mixed - jnp.mean(mixed, axis=-1, keepdims=True)
    normed = (
        centered
        * lax.rsqrt(jnp.mean(centered * centered, axis=-1, keepdims=True) + epsilon)
        * head_gain.reshape(head_count, value_width)
    )
    return (
        jax.nn.silu(gate_rows.astype(jnp.float32))
        * normed.reshape(length, head_count * value_width)
    ).astype(jnp.bfloat16)


def body(
    queries,
    key_rows,
    value_rows,
    gate_rows,
    log_decay,
    head_gain,
    out_weight,
    expert_input,
    input_gain,
    route_ids,
    route_weight,
    expert_gate,
    expert_up,
    expert_down,
):
    hidden = retention_rows(queries, key_rows, value_rows, gate_rows, log_decay, head_gain)
    tp_count = lax.axis_size("tp")
    model_width = out_weight.shape[1]
    mixer_out = lax.psum_scatter(
        jnp.dot(hidden, out_weight, preferred_element_type=jnp.float32).astype(jnp.bfloat16),
        "tp",
        scatter_dimension=0,
        tiled=True,
    )
    token_count = expert_input.shape[0]
    local_experts = expert_gate.shape[0]
    ep_count = lax.axis_size("ep")
    expert_count = ep_count * local_experts
    capacity = 3 * token_count // expert_count
    quarter = model_width // tp_count
    widened = expert_input.astype(jnp.float32)
    normed = (
        widened
        * lax.rsqrt(jnp.mean(widened * widened, axis=-1, keepdims=True) + epsilon)
        * input_gain
    ).astype(jnp.bfloat16)
    flat_ids = route_ids.reshape(-1)
    matches = (flat_ids[:, None] == jnp.arange(expert_count, dtype=jnp.int32)[None, :]).astype(
        jnp.int32
    )
    slot_rank = jnp.sum((jnp.cumsum(matches, axis=0) - matches) * matches, axis=1)
    target = flat_ids * capacity + slot_rank
    owners = jnp.arange(2 * token_count, dtype=jnp.int32) // 2
    slot_table = jnp.full((expert_count * capacity,), token_count, jnp.int32).at[target].set(owners)
    padded = jnp.concatenate([normed, jnp.zeros((1, model_width), jnp.bfloat16)], axis=0)
    outgoing = padded[slot_table].reshape(ep_count, local_experts * capacity, model_width)
    arrived = lax.all_to_all(outgoing, "ep", split_axis=0, concat_axis=0, tiled=True).reshape(
        ep_count, local_experts, capacity, model_width
    )
    gate_val = jnp.einsum(
        "sxcd,xdf->sxcf", arrived, expert_gate, preferred_element_type=jnp.float32
    )
    up_val = jnp.einsum("sxcd,xdf->sxcf", arrived, expert_up, preferred_element_type=jnp.float32)
    inner_rows = (jax.nn.silu(gate_val) * up_val).astype(jnp.bfloat16)
    partial_sum = jnp.einsum(
        "sxcf,xfd->sxcd", inner_rows, expert_down, preferred_element_type=jnp.float32
    )
    summed = lax.psum_scatter(
        partial_sum.astype(jnp.bfloat16), "tp", scatter_dimension=3, tiled=True
    )
    returned = lax.all_to_all(summed, "ep", split_axis=0, concat_axis=0, tiled=True).reshape(
        expert_count * capacity, quarter
    )
    picked = returned[target].reshape(token_count, 2, quarter).astype(jnp.float32)
    expert_out = jnp.sum(picked * route_weight[:, :, None], axis=1).astype(jnp.bfloat16)
    return (mixer_out, expert_out)


def solution(mesh):
    placed = (
        P("ep", "tp"),
        P("ep", "tp"),
        P("ep", "tp"),
        P("ep", "tp"),
        P("tp", "ep"),
        P("tp"),
        P("tp", None),
        P("ep", None),
        P(),
        P("ep", None),
        P("ep", None),
        P("ep", None, "tp"),
        P("ep", None, "tp"),
        P("ep", "tp", None),
    )
    return jax.shard_map(
        body,
        mesh=mesh,
        in_specs=placed,
        out_specs=(P(("ep", "tp"), None), P("ep", "tp")),
        check_vma=False,
    )
```

profile of v0, /device:TPU:0, one launch (start us, length us, event | category | flops | bytes accessed | tf_op | source)
XLA Modules:
  0.0 474.6 jit_solution(17053314373384708201)
XLA Ops:
  8.9 1.2 reduce-window.14
  10.5 1.3 copy.67
  12.6 2.4 copy.95
  15.0 1.4 copy.96
  16.4 1.3 copy.70
  18.6 2.4 copy.97
  20.9 1.3 copy.98
  24.9 4.1 multiply_subtract_fusion
  30.0 1.7 fusion.42
  33.5 9.0 %reduce-window.16 = s32[32,8,128]{2,1,0:T(8,128)S(1)} reduce-window(s32[32,8,128]{2,1,0:T(8,128)S(1)} %fusion.61, s32[]{:T(128)} %constant.96.clone.1), window={size=1x1x128 pad=0_0x0_0x127_0}, to_apply=%region_8.9 | reduce-window | flops 4161536 | bytes 262148 | tf_op jit(solution)/shard_map/reduce-window.2
  44.6 3.2 fusion.1
  47.9 4.8 %scatter_custom_fusion = s32[1536]{0:T(1024)S(1)} fusion(s32[1024]{0:T(1024)S(1)} %bitcast.175, s32[1024]{0:T(1024)S(1)} %add_select_fusion, s32[]{:T(128)} %constant.90.clone.1), kind=kCustom, calls=%fused_computation.94 | custom fusion | bytes 6148 | tf_op jit(solution)/shard_map/scatter | solution.py:161
  52.7 3.8 fusion.3
  56.5 2.5 concatenate.14
  59.0 24.8 %gather_fusion = bf16[1536,4096]{1,0:T(8,128)(2,1)} fusion(bf16[513,4096]{1,0:T(8,128)(2,1)} %concatenate.14, s32[2048]{0:T(1024)S(1)} %pad_clamp_fusion), kind=kCustom, calls=%fused_computation | custom fusion | bytes 25171968 | tf_op jit(solution)/shard_map/gather | solution.py:163
  83.8 149.5 %all_to_all.10 = bf16[32,48,4096]{2,1,0:T(8,128)(2,1)S(1)} all-to-all(bf16[32,48,4096]{2,1,0:T(8,128)(2,1)} %bitcast.156), channel_id=1, replica_groups=mesh['ep'=32,'tp'=4] {'ep'}, dimensions={0} | all-to-all | bytes 25165824 | tf_op jit(solution)/shard_map/all_to_all | solution.py:164
  233.3 4.5 copy-done.4
  237.8 4.7 fusion.18
  242.5 19.5 %convert_bitcast_fusion = bf16[32,1,48,4096]{3,2,0,1:T(8,128)(2,1)} fusion(bf16[1,256,4096]{2,1,0:T(8,128)(2,1)S(1)} %copy-done, bf16[32,48,4096]{2,1,0:T(8,128)(2,1)} %copy-done.4, bf16[1,4096,256]{2,1,0:T(8,128)(2,1)} %param.28, f32[32,48,256]{2,1,0:T(8,128)} %fusion.18), kind=kOutput, calls=%fused_computation.6 | convolution fusion | flops 6451101696 | bytes 30932992 | tf_op jit(solution)/shard_map/sxcf,xfd->sxcd/dot_general | solution.py:172
  264.1 64.9 %all-reduce.1 = bf16[128]{0:T(256)(128)(2,1)S(1)} all-reduce(bf16[128]{0:T(256)(128)(2,1)S(1)} %dynamic-update-slice), channel_id=2, replica_groups=mesh['ep'=32,'tp'=4] {'ep'}, use_global_device_ids=true, to_apply=%add.1 | all-reduce | flops 128 | bytes 512
  329.2 5.4 %fusion.4 = f32[4,512,256]{1,2,0:T(8,128)} fusion(f32[4,512]{1,0:T(4,128)S(1)} %get-tuple-element.143, pred[512,512]{1,0:T(8,128)(4,1)S(1)} %iota_compare_fusion, bf16[64,4,8,256]{3,2,1,0:T(8,128)(2,1)} %bitcast.166, f32[512,4,64]{2,0,1:T(8,128)} %get-tuple-element.148, f32[512,4,64]{2,0,1:T(8,128)} %get-tuple-element.149, f32[512,4,64]{2,0,1:T(8,128)S(1)} %copy-done.6, ...), kind=kOutput, calls=%fused_computation.14 | convolution fusion | flops 811073536 | bytes 5513216 | tf_op jit(solution)/shard_map/hnlm,nmhe->nlhe/dot_general | solution.py:100
  334.6 36.4 %while.9 = (s32[]{:T(128)}, f32[4,128,256]{2,1,0:T(8,128)S(1)}, s32[]{:T(128)}, bf16[32,4]{1,0:T(8,128)(2,1)S(1)}, bf16[32,4,128,256]{3,2,1,0:T(8,128)(2,1)}, /*index=5*/s32[]{:T(128)}, s32[]{:T(128)}) while((s32[]{:T(128)}, f32[4,128,256]{2,1,0:T(8,128)S(1)}, s32[]{:T(128)}, bf16[32,4]{1,0:T(8,128)(2,1)S(1)}, ...), condition=%wide.region_3.4_spmd.clone, body=%wide.region_2.3_spmd.clone.sunk | while | flops 655368 | bytes 1310865 | solution.py:33
  334.6 1.2 fusion.84
  335.9 1.1 fusion.84
  337.0 1.1 fusion.84
  338.1 1.1 fusion.84
  339.3 1.1 fusion.84
  340.4 1.1 fusion.84
  341.5 1.1 fusion.84
  342.7 1.1 fusion.84
  343.8 1.1 fusion.84
  344.9 1.1 fusion.84
  346.1 1.1 fusion.84
  347.2 1.1 fusion.84
  348.4 1.1 fusion.84
  349.5 1.1 fusion.84
  350.6 1.1 fusion.84
  351.8 1.1 fusion.84
  352.9 1.1 fusion.84
  354.0 1.1 fusion.84
  355.2 1.1 fusion.84
  356.3 1.1 fusion.84
  357.4 1.1 fusion.84
  358.6 1.1 fusion.84
  359.7 1.1 fusion.84
  360.8 1.1 fusion.84
  362.0 1.1 fusion.84
  363.1 1.1 fusion.84
  364.3 1.1 fusion.84
  365.4 1.1 fusion.84
  366.5 1.1 fusion.84
  369.9 1.1 fusion.84
  371.1 3.3 fusion.79
  374.3 1.3 copy-done.2
  376.8 1.8 copy.101
  378.6 1.6 sub.70
  380.2 3.1 copy.82
  383.3 1.9 copy.81
  385.2 12.0 %convolution_convert_fusion = bf16[512,4096]{1,0:T(8,128)(2,1)} fusion(bf16[1024,4096]{1,0:T(8,128)(2,1)} %param.22, f32[512,1024]{1,0:T(8,128)} %bitcast.163, f32[512,1024]{1,0:T(8,128)} %copy.81, f32[512,1024]{1,0:T(8,128)} %copy.82, bf16[512,1024]{1,0:T(8,128)(2,1)S(1)} %copy-done.16, f32[1024]{0:T(1024)S(1)} %copy-done.17), kind=kOutput, calls=%fused_computation.12 | convolution fusion | flops 4302307328 | bytes 19927040 | tf_op jit(solution)/shard_map/dot_general | solution.py:137
  397.3 5.1 %all-to-all-start.1 = ((bf16[32,1,48,1024]{3,2,1,0:T(8,128)(2,1)}), bf16[32,1,48,1024]{3,2,1,0:T(8,128)(2,1)}, u32[]{:S(2)}, u32[]{:S(2)}) async-start(bf16[32,1,48,1024]{3,2,1,0:T(8,128)(2,1)} %bitcast.162), calls=%async_computation.3 | async-start | bytes 6291456 | tf_op jit(solution)/shard_map/all_to_all | solution.py:178
  402.5 41.8 %all-to-all-done.1 = bf16[32,1,48,1024]{3,2,1,0:T(8,128)(2,1)} async-done(((bf16[32,1,48,1024]{3,2,1,0:T(8,128)(2,1)}), bf16[32,1,48,1024]{3,2,1,0:T(8,128)(2,1)}, u32[]{:S(2)}, u32[]{:S(2)}) %all-to-all-start.1) | async-done | bytes 3145760 | tf_op jit(solution)/shard_map/all_to_all | solution.py:178
  444.3 8.3 %gather_fusion.1 = bf16[1024,1024]{1,0:T(8,128)(2,1)} fusion(bf16[1536,1024]{1,0:T(8,128)(2,1)} %bitcast.48, s32[1024]{0:T(1024)S(1)} %broadcast_clamp_fusion), kind=kCustom, calls=%fused_computation.1 | custom fusion | bytes 4198400 | tf_op jit(solution)/shard_map/gather | solution.py:181
  452.7 5.6 %reshape.417 = f32[512,2,1024]{2,1,0:T(2,128)} reshape(bf16[1024,1024]{1,0:T(8,128)(2,1)} %gather_fusion.1) | data formatting | bytes 6291456 | tf_op jit(solution)/shard_map/convert_element_type | solution.py:181
  458.3 8.6 %multiply_reduce_fusion = bf16[512,1024]{1,0:T(8,128)(2,1)} fusion(f32[512,2,1024]{2,1,0:T(2,128)} %reshape.417, f32[512,2]{1,0:T(8,128)S(1)} %copy.90), kind=kLoop, calls=%fused_computation.13 | loop fusion | flops 1572864 | bytes 5246976 | tf_op jit(solution)/shard_map/reduce_sum | solution.py:182
  (130 shorter events, 16.0 us)
Async XLA Ops:
  8.0 234.5 %copy-start = (bf16[1,256,4096]{2,1,0:T(8,128)(2,1)S(1)}, bf16[1,256,4096]{2,1,0:T(8,128)(2,1)}, u32[]{:S(2)}) copy-start(bf16[1,256,4096]{2,1,0:T(8,128)(2,1)} %param.29) | copy-start | bytes 6291460
  8.0 326.6 %all-gather.4.cloned.1.call-start = ((), (), s32[]{:S(2)}) async-start(), calls=%async_computation.6 | async-start | bytes 8650752 | tf_op jit(solution)/shard_map/all_gather | solution.py:16
  24.9 5.1 %copy-start.8 = (bf16[512,1024]{1,0:T(8,128)(2,1)S(1)}, bf16[512,1024]{1,0:T(8,128)(2,1)}, u32[]{:S(2)}) copy-start(bf16[512,1024]{1,0:T(8,128)(2,1)} %param.18) | copy-start | bytes 3145732
  29.0 1.0 copy-start.5
  29.0 2.8 copy-start.12
  31.7 365.5 %reduce-scatter.5.cloned.1.call-start = ((), (), s32[]{:S(2)}) async-start(), calls=%async_computation.5 | async-start | bytes 15728640 | tf_op jit(solution)/shard_map/reduce_scatter | solution.py:175
  44.6 3.2 copy-start.10
  44.6 3.2 copy-start.11
  44.6 8.1 %copy-start.9 = (f32[4096]{0:T(1024)S(1)}, f32[4096]{0:T(1024)}, u32[]{:S(2)}) copy-start(f32[4096]{0:T(1024)} %param.24) | copy-start | bytes 49156
  83.8 154.0 %copy-start.15 = (bf16[1,4096,256]{2,1,0:T(8,128)(2,1)S(1)}, bf16[1,4096,256]{2,1,0:T(8,128)(2,1)}, u32[]{:S(2)}) copy-start(bf16[1,4096,256]{2,1,0:T(8,128)(2,1)} %param.27) | copy-start | bytes 6291460
  233.3 4.5 copy-start.4
  262.0 0.7 copy-start.18
  262.0 1.9 copy-start.19
  262.0 67.2 %copy-start.6 = (f32[512,4,64]{2,0,1:T(8,128)S(1)}, f32[512,4,64]{2,0,1:T(8,128)}, u32[]{:S(2)}) copy-start(f32[512,4,64]{2,0,1:T(8,128)} %copy-done.5) | copy-start | bytes 1572868
  262.0 204.8 %reduce-scatter.3.cloned.1.call-start = ((), (), s32[]{:S(2)}) async-start(), calls=%async_computation.4 | async-start | bytes 5242880 | tf_op jit(solution)/shard_map/reduce_scatter | solution.py:136
  334.6 36.4 %copy-start.7 = (f32[512,4,64]{2,0,1:T(8,128)S(1)}, f32[512,4,64]{2,0,1:T(8,128)}, u32[]{:S(2)}) copy-start(f32[512,4,64]{2,0,1:T(8,128)} %get-tuple-element.148) | copy-start | bytes 1572868
  334.6 36.4 %copy-start.14 = (f32[4]{0:T(128)S(1)}, f32[4]{0:T(128)}, u32[]{:S(2)}) copy-start(f32[4]{0:T(128)} %get-tuple-element.140) | copy-start | bytes 52
  374.3 1.4 copy-start.2
  380.2 3.1 copy-start.3
  383.3 1.9 copy-start.16
  383.3 1.9 copy-start.17
  397.3 5.1 %copy-start.13 = (f32[512,2]{0,1:T(2,128)S(1)}, f32[512,2]{0,1:T(2,128)}, u32[]{:S(2)}) copy-start(f32[512,2]{0,1:T(2,128)} %param.26) | copy-start | bytes 12292
  397.3 47.1 %all-to-all-start.1 = ((bf16[32,1,48,1024]{3,2,1,0:T(8,128)(2,1)}), bf16[32,1,48,1024]{3,2,1,0:T(8,128)(2,1)}, u32[]{:S(2)}, u32[]{:S(2)}) async-start(bf16[32,1,48,1024]{3,2,1,0:T(8,128)(2,1)} %bitcast.162), calls=%async_computation.3 | async-start | bytes 6291456 | tf_op jit(solution)/shard_map/all_to_all | solution.py:178
  452.7 14.2 %copy-start.1 = (bf16[1,256,4096]{2,1,0:T(8,128)(2,1)S(1)}, bf16[1,256,4096]{2,1,0:T(8,128)(2,1)}, u32[]{:S(2)}) copy-start(bf16[1,256,4096]{2,1,0:T(8,128)(2,1)} %param.29) | copy-start | bytes 6291460
Sparse Core Ops, SparseCore 0:
  31.9 55.3 all-gather.3
Sparse Core Ops, SparseCore 1:
  262.1 112.4 reduce-scatter.4
  397.3 43.0 reduce-scatter.2
where the time goes:
time: 482 us; the launch traced here: 475 us
  blocking collectives  214 us (44%)
  local copies, waits for them, and re-layouts  79.8 us (17%)
  other arithmetic  69 us (14%)
  matrix products  46.6 us (10%)
  waiting for transfers between devices  41.9 us (9%)
  between operations  16.7 us (3%)
  starting transfers between devices  5.19 us (1%)
    all_to_all x1, blocking collectives, body(): lax.all_to_all(outgoing, 'ep', split_axis=0, concat_axis=0, tiled=True)  149 us
    unnamed x1, blocking collectives  64.9 us
    all_to_all x1, waiting for transfers between devices, body(): lax.all_to_all(summed, 'ep', split_axis=0, concat_axis=0, tiled=True)  41.8 us
    select_n x32, other arithmetic, hop(): return jax.tree.map(lambda a, b: jnp.where(reached, a, b), new, before)  35.1 us
    gather x1, local copies, waits for them, and re-layouts, body(): padded[slot_table].reshape(ep_count, local_experts * capacity, model_width)  24.8 us
    unnamed x52, local copies, waits for them, and re-layouts  20.3 us
    dot_general x1, matrix products, body(): jnp.einsum('sxcf,xfd->sxcd', inner_rows, expert_down, preferred_element_t...  19.5 us
    dot_general x1, matrix products, body(): jnp.dot(hidden, out_weight, preferred_element_type=jnp.float32)  12 us
  transfers between devices with their start and end apart: 4, of which 1 were waited for; matrix products, arithmetic and copies ran while one was open for 35% of the time, Pallas kernels for 0%

commit v1 on v0

--- a/solution.py
+++ b/solution.py
@@ -1,6 +1,8 @@
 import jax
 import jax.numpy as jnp
 from jax import lax
+from jax.experimental import pallas as pl
+from jax.experimental.pallas import tpu as pltpu
 from jax.sharding import PartitionSpec as P
 
 BLOCK = 512
@@ -112,6 +114,264 @@
         jax.nn.silu(gate_rows.astype(jnp.float32))
         * normed.reshape(length, head_count * value_width)
     ).astype(jnp.bfloat16)
+
+
+ROWS = 256
+CHUNKS = 4
+QUARTER = 1024
+MESH = pl.DeviceIdType.MESH
+
+
+def moe_kernel(
+    packed, meta, gate_w, up_w, down_w, mix_hi, mix_lo, out,
+    recv, meta_in, wg, wu, wd, inner, part, fwd_l, fwd_r, sum_r, sum_l, in_l, in_r, res, ret, acc,
+    d_send, d_recv, m_send, m_recv, own_sem, w_send, w_recv, w_own, x_send, x_recv, r_send, r_recv, r_own,
+):
+    ep, tp = lax.axis_index("ep"), lax.axis_index("tp")
+    core, chip = ep % 2, ep // 2
+    z, y = chip // 4, chip % 4
+    right, left = (tp + 1) % 4, (tp + 3) % 4
+    far = (tp + 2) % 4
+
+    def chip_at(dz, dy):
+        return ((z + dz) % 4) * 4 + (y + dy) % 4
+
+    def rows_of(c):
+        return pl.ds(pl.multiple_of(c * 16, 16), 16)
+
+    barrier = pltpu.get_barrier_semaphore()
+    for dz, dy in HOPS:
+        pl.semaphore_signal(barrier, inc=1, device_id=(chip_at(dz, dy) * 2 + core, tp), device_id_type=MESH)
+    for t in (left, right):
+        pl.semaphore_signal(barrier, inc=1, device_id=(ep, t), device_id_type=MESH)
+    pl.semaphore_signal(barrier, inc=1, device_id=(chip * 2 + 1 - core, tp), device_id_type=MESH)
+    pl.semaphore_wait(barrier, len(HOPS) + 3)
+
+    metas, sends = [], []
+    for i, (dz, dy) in enumerate(HOPS):
+        t = chip_at(dz, dy)
+        c = pltpu.make_async_remote_copy(
+            src_ref=meta.at[rows_of(t)], dst_ref=meta_in.at[rows_of(chip)],
+            send_sem=m_send.at[i], recv_sem=m_recv.at[i],
+            device_id=(t * 2 + core, tp), device_id_type=MESH)
+        c.start()
+        metas.append(c)
+    for k in range(CHUNKS):
+        row = []
+        for i, (dz, dy) in enumerate(HOPS):
+            t = chip_at(dz, dy)
+            c = pltpu.make_async_remote_copy(
+                src_ref=packed.at[k, rows_of(t)], dst_ref=recv.at[k, rows_of(chip)],
+                send_sem=d_send.at[k, i], recv_sem=d_recv.at[k, i],
+                device_id=(t * 2 + core, tp), device_id_type=MESH)
+            c.start()
+            row.append(c)
+        sends.append(row)
+    weights = []
+    for i, (a, b) in enumerate(((gate_w, wg), (up_w, wu), (down_w, wd))):
+        c = pltpu.make_async_remote_copy(
+            src_ref=a, dst_ref=b.at[core], send_sem=w_send.at[i], recv_sem=w_recv.at[i],
+            device_id=(chip * 2 + 1 - core, tp), device_id_type=MESH)
+        c.start()
+        own = pltpu.make_async_copy(a, b.at[core], w_own.at[i])
+        own.start()
+        weights.append((c, own))
+    owns = []
+    for k in range(CHUNKS):
+        c = pltpu.make_async_copy(packed.at[k, rows_of(chip)], recv.at[k, rows_of(chip)], own_sem.at[k])
+        c.start()
+        owns.append(c)
+    c = pltpu.make_async_copy(meta.at[rows_of(chip)], meta_in.at[rows_of(chip)], own_sem.at[CHUNKS])
+    c.start()
+    owns.append(c)
+
+    def x_copy(src, dst, slot, k, to):
+        return pltpu.make_async_remote_copy(
+            src_ref=src, dst_ref=dst, send_sem=x_send.at[slot, k], recv_sem=x_recv.at[slot, k],
+            device_id=(ep, to), device_id_type=MESH)
+
+    top, low = pl.ds(0, 128), pl.ds(128, 128)
+    pending = []
+
+    def launch(c):
+        c.start()
+        pending.append(c)
+        return c
+
+    xs = {}
+    returns = {}
+
+    def compute(k):
+        kinds = ((0,), (0, 1), (0, 1), (1,))[k]
+        if len(kinds) == 2:
+            lane = lax.broadcasted_iota(jnp.int32, (ROWS, 128), 1)
+            is_even = jnp.sum(jnp.where(lane == k, meta_in[...].astype(jnp.float32), 0.0), axis=1, keepdims=True) > 0.5
+        for e in kinds:
+            x = recv[k]
+            g = jnp.dot(x, wg[e], preferred_element_type=jnp.float32)
+            u = jnp.dot(x, wu[e], preferred_element_type=jnp.float32)
+            h = g / (1.0 + jnp.exp(-g)) * u
+            if len(kinds) == 2:
+                h = jnp.where(is_even, h, 0.0) if e == 0 else jnp.where(is_even, 0.0, h)
+            inner[e] = h.astype(jnp.bfloat16)
+
+        def quarter(q):
+            def half(n, carry):
+                cols = pl.ds(pl.multiple_of(q * QUARTER + n * 512, 512), 512)
+                total = None
+                for e in kinds:
+                    d = jnp.dot(inner[e], wd[e, :, cols], preferred_element_type=jnp.float32)
+                    total = d if total is None else total + d
+                part[k, q, :, pl.ds(pl.multiple_of(n * 512, 512), 512)] = total.astype(jnp.bfloat16)
+                return carry
+
+            lax.fori_loop(0, 2, half, 0)
+
+        quarter(far)
+        xs[k, 0] = launch(x_copy(part.at[k, far, top], fwd_l.at[k], 0, k, right))
+        xs[k, 1] = launch(x_copy(part.at[k, far, low], fwd_r.at[k], 1, k, left))
+        quarter(right)
+        xs[k, 2] = launch(x_copy(part.at[k, right, low], in_l.at[k, low], 2, k, right))
+        quarter(left)
+        xs[k, 3] = launch(x_copy(part.at[k, left, top], in_r.at[k, top], 3, k, left))
+        quarter(tp)
+
+    def forward(k):
+        xs[k, 0].wait_recv()
+        sum_r[k] = (fwd_l[k].astype(jnp.float32) + part[k, right, top].astype(jnp.float32)).astype(jnp.bfloat16)
+        xs[k, 4] = launch(x_copy(sum_r.at[k], in_l.at[k, top], 4, k, right))
+        xs[k, 1].wait_recv()
+        sum_l[k] = (fwd_r[k].astype(jnp.float32) + part[k, left, low].astype(jnp.float32)).astype(jnp.bfloat16)
+        xs[k, 5] = launch(x_copy(sum_l.at[k], in_r.at[k, low], 5, k, left))
+
+    def finish(k):
+        for s in (2, 3, 4, 5):
+            xs[k, s].wait_recv()
+        res[k] = (
+            part[k, tp].astype(jnp.float32) + in_l[k].astype(jnp.float32) + in_r[k].astype(jnp.float32)
+        ).astype(jnp.bfloat16)
+        row = []
+        for i, (dz, dy) in enumerate(HOPS):
+            t = chip_at(dz, dy)
+            c = pltpu.make_async_remote_copy(
+                src_ref=res.at[k, rows_of(t)], dst_ref=ret.at[k, rows_of(chip)],
+                send_sem=r_send.at[k, i], recv_sem=r_recv.at[k, i],
+                device_id=(t * 2 + core, tp), device_id_type=MESH)
+            row.append(launch(c))
+        mine = pltpu.make_async_copy(res.at[k, rows_of(chip)], ret.at[k, rows_of(chip)], r_own.at[k])
+        mine.start()
+        returns[k] = (row, mine)
+
+    def combine(k):
+        row, mine = returns[k]
+        for c in row:
+            c.wait_recv()
+        mine.wait()
+        cols = pl.ds(k * ROWS, ROWS)
+        for n in range(2):
+            f = pl.ds(n * 512, 512)
+            part_sum = jnp.dot(mix_hi[:, cols], ret[k, :, f], preferred_element_type=jnp.float32)
+            part_sum = part_sum + jnp.dot(mix_lo[:, cols], ret[k, :, f], preferred_element_type=jnp.float32)
+            if k == 0:
+                acc[:, f] = part_sum
+            elif k < CHUNKS - 1:
+                acc[:, f] += part_sum
+            else:
+                out[:, f] = (acc[:, f] + part_sum).astype(jnp.bfloat16)
+
+    for c, own in weights:
+        own.wait()
+        c.wait_recv()
+    owns[CHUNKS].wait()
+    for c in metas:
+        c.wait_recv()
+    for k in range(CHUNKS):
+        for c in sends[k]:
+            c.wait_recv()
+        owns[k].wait()
+        compute(k)
+        if k > 0:
+            finish(k - 1)
+        forward(k)
+        if k > 1:
+            combine(k - 2)
+    combine(CHUNKS - 2)
+    finish(CHUNKS - 1)
+    combine(CHUNKS - 1)
+    for c, own in weights:
+        c.wait_send()
+    for c in metas:
+        c.wait_send()
+    for row in sends:
+        for c in row:
+            c.wait_send()
+    for c in pending:
+        c.wait_send()
+
+
+HOPS = (
+    (1, 0), (0, 1), (3, 0), (0, 3), (1, 1), (3, 3), (1, 3), (3, 1),
+    (2, 0), (0, 2), (2, 1), (1, 2), (2, 3), (3, 2), (2, 2),
+)
+
+
+def routed(normed, route_ids, route_weight, gate_w, up_w, down_w):
+    tokens, width = normed.shape
+    experts = 32
+    kinds = jnp.arange(experts, dtype=jnp.int32)
+    one_hot = route_ids[:, :, None] == kinds[None, None, :]
+    named = jnp.any(one_hot, axis=1).astype(jnp.bfloat16)
+    steps = jnp.arange(tokens, dtype=jnp.int32)
+    earlier = (steps[:, None] > steps[None, :]).astype(jnp.bfloat16)
+    rank = jnp.dot(earlier, named, preferred_element_type=jnp.float32).astype(jnp.int32)
+    slot = jnp.where(kinds % 2 == 0, rank, 63 - rank)
+    place = (slot // 16) * ROWS + (kinds // 2) * 16 + slot % 16
+    spot = jnp.sum(jnp.where(one_hot, place[:, None, :], 0), axis=2)
+    entries = jnp.arange(CHUNKS * ROWS, dtype=jnp.int32)
+    chosen = (entries[:, None] == spot[:, 0][None, :]) | (entries[:, None] == spot[:, 1][None, :])
+    packed = jnp.dot(chosen.astype(jnp.bfloat16), normed, preferred_element_type=jnp.float32).astype(jnp.bfloat16)
+    mix = jnp.where(entries[None, :] == spot[:, 0:1], route_weight[:, 0:1], 0.0) + jnp.where(
+        entries[None, :] == spot[:, 1:2], route_weight[:, 1:2], 0.0
+    )
+    rounded = lax.reduce_precision(mix, 8, 7)
+    mix_hi = rounded.astype(jnp.bfloat16)
+    mix_lo = (mix - rounded).astype(jnp.bfloat16)
+    even_count = jnp.sum(named.astype(jnp.float32), axis=0)[0::2].astype(jnp.int32)
+    slots = jnp.arange(16, dtype=jnp.int32)[None, :, None] + 16 * jnp.arange(128, dtype=jnp.int32)[None, None, :]
+    meta = (slots < even_count[:, None, None]).astype(jnp.bfloat16).reshape(256, 128)
+    any_space, vmem = pl.BlockSpec(memory_space=pl.ANY), pl.BlockSpec(memory_space=pltpu.VMEM)
+    bf = jnp.bfloat16
+    dma = pltpu.SemaphoreType.DMA
+    return pl.pallas_call(
+        moe_kernel,
+        out_shape=jax.ShapeDtypeStruct((tokens, QUARTER), bf),
+        in_specs=[any_space, any_space, any_space, any_space, any_space, vmem, vmem],
+        out_specs=vmem,
+        scratch_shapes=[
+            pltpu.VMEM((CHUNKS, ROWS, width), bf),
+            pltpu.VMEM((256, 128), bf),
+            pltpu.VMEM((2, width, 256), bf),
+            pltpu.VMEM((2, width, 256), bf),
+            pltpu.VMEM((2, 256, width), bf),
+            pltpu.VMEM((2, ROWS, 256), bf),
+            pltpu.VMEM((CHUNKS, 4, ROWS, QUARTER), bf),
+            pltpu.VMEM((CHUNKS, 128, QUARTER), bf),
+            pltpu.VMEM((CHUNKS, 128, QUARTER), bf),
+            pltpu.VMEM((CHUNKS, 128, QUARTER), bf),
+            pltpu.VMEM((CHUNKS, 128, QUARTER), bf),
+            pltpu.VMEM((CHUNKS, ROWS, QUARTER), bf),
+            pltpu.VMEM((CHUNKS, ROWS, QUARTER), bf),
+            pltpu.VMEM((CHUNKS, ROWS, QUARTER), bf),
+            pltpu.VMEM((CHUNKS, ROWS, QUARTER), bf),
+            pltpu.VMEM((tokens, QUARTER), jnp.float32),
+            dma((CHUNKS, 15)), dma((CHUNKS, 15)), dma((15,)), dma((15,)), dma((CHUNKS + 1,)),
+            dma((3,)), dma((3,)), dma((3,)), dma((6, CHUNKS)), dma((6, CHUNKS)),
+            dma((CHUNKS, 15)), dma((CHUNKS, 15)), dma((CHUNKS,)),
+        ],
+        compiler_params=pltpu.CompilerParams(
+            collective_id=0, has_side_effects=True, vmem_limit_bytes=60 * 1024 * 1024
+        ),
+    )(packed.reshape(CHUNKS, ROWS, width), meta, gate_w[0], up_w[0], down_w[0], mix_hi, mix_lo)
 
 
 def body(
@@ -131,55 +391,19 @@
     expert_down,
 ):
     hidden = retention_rows(queries, key_rows, value_rows, gate_rows, log_decay, head_gain)
-    tp_count = lax.axis_size("tp")
-    model_width = out_weight.shape[1]
     mixer_out = lax.psum_scatter(
         jnp.dot(hidden, out_weight, preferred_element_type=jnp.float32).astype(jnp.bfloat16),
         "tp",
         scatter_dimension=0,
         tiled=True,
     )
-    token_count = expert_input.shape[0]
-    local_experts = expert_gate.shape[0]
-    ep_count = lax.axis_size("ep")
-    expert_count = ep_count * local_experts
-    capacity = 3 * token_count // expert_count
-    quarter = model_width // tp_count
     widened = expert_input.astype(jnp.float32)
     normed = (
         widened
         * lax.rsqrt(jnp.mean(widened * widened, axis=-1, keepdims=True) + epsilon)
         * input_gain
     ).astype(jnp.bfloat16)
-    flat_ids = route_ids.reshape(-1)
-    matches = (flat_ids[:, None] == jnp.arange(expert_count, dtype=jnp.int32)[None, :]).astype(
-        jnp.int32
-    )
-    slot_rank = jnp.sum((jnp.cumsum(matches, axis=0) - matches) * matches, axis=1)
-    target = flat_ids * capacity + slot_rank
-    owners = jnp.arange(2 * token_count, dtype=jnp.int32) // 2
-    slot_table = jnp.full((expert_count * capacity,), token_count, jnp.int32).at[target].set(owners)
-    padded = jnp.concatenate([normed, jnp.zeros((1, model_width), jnp.bfloat16)], axis=0)
-    outgoing = padded[slot_table].reshape(ep_count, local_experts * capacity, model_width)
-    arrived = lax.all_to_all(outgoing, "ep", split_axis=0, concat_axis=0, tiled=True).reshape(
-        ep_count, local_experts, capacity, model_width
-    )
-    gate_val = jnp.einsum(
-        "sxcd,xdf->sxcf", arrived, expert_gate, preferred_element_type=jnp.float32
-    )
-    up_val = jnp.einsum("sxcd,xdf->sxcf", arrived, expert_up, preferred_element_type=jnp.float32)
-    inner_rows = (jax.nn.silu(gate_val) * up_val).astype(jnp.bfloat16)
-    partial_sum = jnp.einsum(
-        "sxcf,xfd->sxcd", inner_rows, expert_down, preferred_element_type=jnp.float32
-    )
-    summed = lax.psum_scatter(
-        partial_sum.astype(jnp.bfloat16), "tp", scatter_dimension=3, tiled=True
-    )
-    returned = lax.all_to_all(summed, "ep", split_axis=0, concat_axis=0, tiled=True).reshape(
-        expert_count * capacity, quarter
-    )
-    picked = returned[target].reshape(token_count, 2, quarter).astype(jnp.float32)
-    expert_out = jnp.sum(picked * route_weight[:, :, None], axis=1).astype(jnp.bfloat16)
+    expert_out = routed(normed, route_ids, route_weight, expert_gate, expert_up, expert_down)
     return (mixer_out, expert_out)
 
 

time: 482 us -> 337 us (0.70); the launches traced: 475 us -> 336 us
  Pallas kernels: 0 us -> 150 us
  blocking collectives: 214 us -> 69.8 us
  local copies, waits for them, and re-layouts: 79.8 us -> 21.3 us
  waiting for transfers between devices: 41.9 us -> 0.06 us
  other arithmetic: 69 us -> 48.4 us
  matrix products: 46.6 us -> 30.7 us
  starting transfers between devices: 5.19 us -> 0.08 us
    pallas_call x0 -> x1, Pallas kernels: none -> 150 us  [routed(): pl.pallas_call(moe_kernel, out_shape=jax.ShapeDtypeStruct((tokens, QUARTE...]
    all_to_all x1 -> x0, blocking collectives: 149 us -> none  [body(): lax.all_to_all(outgoing, 'ep', split_axis=0, concat_axis=0, tiled=True)]
    all_to_all x1 -> x0, waiting for transfers between devices: 41.8 us -> none  [body(): lax.all_to_all(summed, 'ep', split_axis=0, concat_axis=0, tiled=True)]
    gather x2 -> x0, local copies, waits for them, and re-layouts: 33.1 us -> none  [the longest x1 24.8 us: body(): padded[slot_table].reshape(ep_count, local_experts * capacity, model_width)]
    dot_general x2, matrix products: 24.2 us -> 7.65 us  [the longest x1 7.36 us: routed(): jnp.dot(chosen.astype(jnp.bfloat16), normed, preferred_element_type=jnp.f...]
    another operation x5 -> x2, other arithmetic: 10.5 us -> 1.38 us
    reduce_sum x2, other arithmetic: 8.62 us -> 0.15 us  [the longest x1 0.11 us: routed(): jnp.sum(named.astype(jnp.float32), axis=0)[0::2].astype(jnp.int32)]
    unnamed x52 -> x27, local copies, waits for them, and re-layouts: 20.3 us -> 12.4 us
  transfers between devices with their start and end apart: 4 -> 2, of which waited for: 1 -> 0; matrix products, arithmetic and copies ran while one was open for 35% -> 6% of each run, Pallas kernels for 0% -> 45%
where the time goes in v1:
time: 337 us; the launch traced here: 336 us
  Pallas kernels  150 us (45%)
  blocking collectives  69.8 us (21%)
  other arithmetic  48.4 us (14%)
  matrix products  30.7 us (9%)
  local copies, waits for them, and re-layouts  21.3 us (6%)
  between operations  14.9 us (4%)
    pallas_call x1, Pallas kernels, routed(): pl.pallas_call(moe_kernel, out_shape=jax.ShapeDtypeStruct((tokens, QUARTE...  150 us
    unnamed x1, blocking collectives  69.8 us
    select_n x32, other arithmetic, hop(): return jax.tree.map(lambda a, b: jnp.where(reached, a, b), new, before)  34.9 us
    unnamed x27, local copies, waits for them, and re-layouts  12.4 us
    dot_general x1, matrix products, body(): jnp.dot(hidden, out_weight, preferred_element_type=jnp.float32)  12.3 us
    dot_general x1, matrix products, routed(): jnp.dot(chosen.astype(jnp.bfloat16), normed, preferred_element_type=jnp.f...  7.36 us
  transfers between devices with their start and end apart: 2, of which 0 were waited for; matrix products, arithmetic and copies ran while one was open for 6% of the time, Pallas kernels for 45%

profile of v1, /device:TPU:0, one launch (start us, length us, event | category | flops | bytes accessed | tf_op | source)
XLA Modules:
  0.0 335.9 jit_solution(12518602543669200832)
XLA Ops:
  7.2 0.7 reshape.371
  7.9 1.2 reduce-window.6
  9.5 1.3 copy.78
  10.9 1.4 copy.100
  12.3 0.2 copy.81
  12.6 1.3 copy.101
  13.9 1.3 copy.102
  15.2 1.3 copy.99
  17.0 1.0 multiply_cosine_fusion
  18.1 4.1 %multiply_subtract_fusion = (f32[512,4,64]{2,0,1:T(8,128)S(1)}, f32[512,4,64]{2,0,1:T(8,128)S(1)}, f32[512,4,64]{2,0,1:T(8,128)}, f32[512,4,64]{2,0,1:T(8,128)}) fusion(f32[512,4,64]{2,0,1:T(8,128)} %copy.102, f32[512,4,64]{2,0,1:T(8,128)} %copy.101, f32[512,64]{1,0:T(8,128)S(1)} %get-tuple-element.161, f32[512,64]{1,0:T(8,128)S(1)} %get-tuple-element.160, ...), kind=kLoop, calls=%fused_computation.60 | loop fusion | flops 1572864 | bytes 4456448 | tf_op jit(solution)/shard_map/sub | solution.py:47
  22.2 1.8 fusion.34
  24.1 0.6 dynamic-slice.1
  25.2 0.2 dynamic-update-slice
  25.5 69.8 %all-reduce = bf16[128]{0:T(256)(128)(2,1)S(1)} all-reduce(bf16[128]{0:T(256)(128)(2,1)S(1)} %dynamic-update-slice), channel_id=2, replica_groups=mesh['ep'=32,'tp'=4] {'ep'}, use_global_device_ids=true, to_apply=%add | all-reduce | flops 128 | bytes 512
  95.5 5.4 %fusion.7 = f32[4,512,256]{1,2,0:T(8,128)} fusion(f32[4,512]{1,0:T(4,128)S(1)} %get-tuple-element.143, pred[512,512]{1,0:T(8,128)(4,1)S(1)} %iota_compare_fusion.6, bf16[64,4,8,256]{3,2,1,0:T(8,128)(2,1)} %bitcast.95, f32[512,4,64]{2,0,1:T(8,128)} %get-tuple-element.148, f32[512,4,64]{2,0,1:T(8,128)} %get-tuple-element.149, ...), kind=kOutput, calls=%fused_computation.12 | convolution fusion | flops 811073536 | bytes 5513216 | tf_op jit(solution)/shard_map/hnlm,nmhe->nlhe/dot_general | solution.py:102
  100.9 36.2 %while.9 = (s32[]{:T(128)}, f32[4,128,256]{2,1,0:T(8,128)S(1)}, s32[]{:T(128)}, bf16[32,4]{1,0:T(8,128)(2,1)S(1)}, bf16[32,4,128,256]{3,2,1,0:T(8,128)(2,1)}, /*index=5*/s32[]{:T(128)}, s32[]{:T(128)}) while((s32[]{:T(128)}, f32[4,128,256]{2,1,0:T(8,128)S(1)}, s32[]{:T(128)}, bf16[32,4]{1,0:T(8,128)(2,1)S(1)}, ...), condition=%wide.region_3.4_spmd.clone, body=%wide.region_2.3_spmd.clone.sunk | while | flops 655368 | bytes 1310865 | solution.py:35
  100.9 1.1 fusion.78
  102.0 1.1 fusion.78
  103.2 1.1 fusion.78
  104.3 1.1 fusion.78
  105.4 1.1 fusion.78
  106.6 1.1 fusion.78
  107.7 1.1 fusion.78
  108.8 1.1 fusion.78
  110.0 1.1 fusion.78
  111.1 1.1 fusion.78
  112.2 1.1 fusion.78
  113.4 1.1 fusion.78
  114.5 1.1 fusion.78
  115.6 1.1 fusion.78
  116.8 1.1 fusion.78
  117.9 1.1 fusion.78
  119.0 1.1 fusion.78
  120.1 1.1 fusion.78
  121.3 1.1 fusion.78
  122.4 1.1 fusion.78
  123.5 1.1 fusion.78
  124.7 1.1 fusion.78
  125.8 1.1 fusion.78
  126.9 1.1 fusion.78
  128.1 1.1 fusion.78
  129.2 1.1 fusion.78
  130.3 1.1 fusion.78
  131.5 1.1 fusion.78
  132.6 1.1 fusion.78
  133.7 1.1 fusion.78
  134.9 1.1 fusion.78
  136.0 1.1 fusion.78
  137.1 3.6 %fusion.74 = (f32[512,4]{0,1:T(4,128)S(1)}, f32[1,512,4,256]{1,3,2,0:T(8,128)S(1)}) fusion(f32[4,128,256]{2,1,0:T(8,128)S(1)} %get-tuple-element.111, f32[4]{0:T(128)S(1)} %get-tuple-element.140, f32[4,512]{1,0:T(4,128)S(1)} %get-tuple-element.142, f32[512,4,64]{2,0,1:T(8,128)} %get-tuple-element.148, f32[512,4,64]{2,0,1:T(8,128)} %get-tuple-element.149, ...), kind=kOutput, calls=%fused_computation.124 | convolution fusion | flops 135919616 | bytes 5783568 | tf_op jit(solution)/shard_map/nlhd,hnl,nhde->nlhe/dot_general | solution.py:105
  140.7 0.3 fusion.20
  141.2 0.6 mul.243
  141.8 1.8 copy.105
  143.6 1.6 sub.82
  145.2 2.9 copy.93
  148.1 1.9 copy.92
  149.9 12.3 %convolution_convert_fusion.1 = bf16[512,4096]{1,0:T(8,128)(2,1)} fusion(bf16[1024,4096]{1,0:T(8,128)(2,1)} %param.22, f32[512,1024]{1,0:T(8,128)} %bitcast.92, f32[512,1024]{1,0:T(8,128)} %copy.92, f32[512,1024]{1,0:T(8,128)} %copy.93, bf16[512,1024]{1,0:T(8,128)(2,1)} %param.19, f32[1024]{0:T(1024)S(1)} %copy-done.6), kind=kOutput, calls=%fused_computation.9 | convolution fusion | flops 4302307328 | bytes 19927040 | tf_op jit(solution)/shard_map/dot_general | solution.py:395
  162.3 0.7 copy-done.3
  163.4 0.7 fusion.51.meta
  164.1 0.3 fusion.54
  164.5 3.2 fusion.1
  167.7 2.0 fusion.18
  169.7 7.4 %convolution_convert_fusion = bf16[1024,4096]{1,0:T(8,128)(2,1)} fusion(bf16[512,4096]{1,0:T(8,128)(2,1)S(1)} %copy-done, f32[4096]{0:T(1024)S(1)} %copy-done.5, f32[512]{0:T(512)S(1)} %add_rsqrt_fusion.1, s32[512]{0:T(512)S(1)} %bitcast.105, s32[512]{0:T(512)S(1)} %bitcast.103), kind=kOutput, calls=%fused_computation.8 | convolution fusion | flops 4309123072 | bytes 12605440 | tf_op jit(solution)/shard_map/dot_general | solution.py:332
  177.1 149.7 %shard_map.149 = bf16[512,1024]{1,0:T(8,128)(2,1)} custom-call(bf16[4,256,4096]{2,1,0:T(8,128)(2,1)} %bitcast.84, bf16[256,128]{1,0:T(8,128)(2,1)} %fusion.51.meta, bf16[4096,256]{1,0:T(8,128)(2,1)} %bitcast.89, bf16[4096,256]{1,0:T(8,128)(2,1)} %bitcast.90, bf16[256,4096]{1,0:T(8,128)(2,1)} %bitcast.91, bf16[512,1024]{1,0:T(8,128)(2,1)} %get-tuple-element.155.mix_hi, ...), custom_call_target="tpu_custom_call" | custom-call | tf_op jit(solution)/shard_map/pallas_call | solution.py:345
  326.8 2.3 copy.124
  (89 shorter events, 2.4 us)
Async XLA Ops:
  7.2 93.7 %all-gather.4.cloned.1.call-start = ((), (), s32[]{:S(2)}) async-start(), calls=%async_computation.2 | async-start | bytes 8650752 | tf_op jit(solution)/shard_map/all_gather | solution.py:18
  10.7 1.5 copy-start.2
  18.1 4.1 %copy-start.1 = (bf16[512,1024]{1,0:T(8,128)(2,1)S(1)}, bf16[512,1024]{1,0:T(8,128)(2,1)}, u32[]{:S(2)}) copy-start(bf16[512,1024]{1,0:T(8,128)(2,1)} %param.18) | copy-start | bytes 3145732
  22.2 1.9 copy-start.7
  24.0 302.8 %reduce-scatter.2.cloned.1.call-start = ((), (), s32[]{:S(2)}) async-start(), calls=%async_computation.1 | async-start | bytes 5242880 | tf_op jit(solution)/shard_map/reduce_scatter | solution.py:394
  148.1 1.9 copy-start.6
  162.2 0.7 copy-start.3
  164.4 3.3 copy-start.4
  164.4 5.3 %copy-start = (bf16[512,4096]{1,0:T(8,128)(2,1)S(1)}, bf16[512,4096]{1,0:T(8,128)(2,1)}, u32[]{:S(2)}) copy-start(bf16[512,4096]{1,0:T(8,128)(2,1)} %param.23) | copy-start | bytes 12582916
  167.7 2.0 copy-start.5
Sparse Core Ops, SparseCore 0:
  24.1 55.5 all-gather.3
  162.4 43.0 reduce-scatter.1

commit v2 on v1

--- a/solution.py
+++ b/solution.py
@@ -5,115 +5,69 @@
 from jax.experimental.pallas import tpu as pltpu
 from jax.sharding import PartitionSpec as P
 
-BLOCK = 512
-
 
 epsilon = 1e-06
 theta_base = 10000.0
 
-
-def prefix(value, axis, combine, identity):
-    length, index = (lax.axis_size(axis), lax.axis_index(axis))
-    everything = jax.tree.map(
-        lambda part, kind: lax.all_gather(part.astype(kind), axis),
-        value,
-        (jnp.bfloat16, jnp.bfloat16),
-    )
-    start = jax.tree.map(
-        lambda part, zero: jnp.broadcast_to(jnp.asarray(zero, part.dtype), part.shape),
-        value,
-        identity,
-    )
-
-    def hop(k, before):
-        reached = k < index
-        new = combine(
-            before, jax.tree.map(lambda part, own: part[k].astype(own.dtype), everything, value)
+def local_kernel(queries, key_rows, value_rows, cosine, sine, run_cols, run_rows, inside, scaled, state, keys, mixed_q):
+    half = 64
+    for h in range(4):
+        cols, vals = pl.ds(h * 128, 128), pl.ds(h * 256, 256)
+        q = queries[:, cols].astype(jnp.float32)
+        k = key_rows[:, cols].astype(jnp.float32)
+        q = q * cosine[...] + pltpu.roll(q, half, 1) * sine[...]
+        k = (k * cosine[...] + pltpu.roll(k, half, 1) * sine[...]) * 128.0 ** (-0.5)
+        run = run_cols[:, h : h + 1]
+        ending = run_rows[h : h + 1, 511:512]
+        keys[...] = k.astype(jnp.bfloat16)
+        mixed_q[...] = q.astype(jnp.bfloat16)
+        scaled[:, cols] = (q * jnp.exp(run)).astype(jnp.bfloat16)
+        kept = (k * jnp.exp(ending - run)).astype(jnp.bfloat16)
+        state[pl.ds(h * 128, 128), :] = lax.dot_general(
+            kept, value_rows[:, vals], (((0,), (0,)), ((), ())), preferred_element_type=jnp.float32
         )
-        return jax.tree.map(lambda a, b: jnp.where(reached, a, b), new, before)
-
-    return lax.fori_loop(0, length, hop, start)
-
-
-def rotate(values, positions):
-    half_dim = values.shape[-1] // 2
-    frequency = theta_base ** (-jnp.arange(half_dim, dtype=jnp.float32) / half_dim)
-    angles = positions.astype(jnp.float32)[:, None, None] * frequency
-    cosine = jnp.cos(angles)
-    sine_wave = jnp.sin(angles)
-    first_half = values[..., :half_dim]
-    second = values[..., half_dim:]
-    return jnp.concatenate(
-        [first_half * cosine - second * sine_wave, second * cosine + first_half * sine_wave],
-        axis=-1,
-    )
-
-
-def to_blocks(array, blocks):
-    return array.reshape(blocks, array.shape[0] // blocks, array.shape[1], array.shape[2])
-
-
-def combine_states(earlier, later):
-    return (later[1][:, None, None] * earlier[0] + later[0], earlier[1] * later[1])
-
-
-def retention_rows(queries, key_rows, value_rows, gate_rows, log_decay, head_gain):
+        for b in range(4):
+            rows, wide = pl.ds(b * 128, 128), (b + 1) * 128
+            scores = lax.dot_general(
+                mixed_q[rows, :], keys[pl.ds(0, wide), :], (((1,), (1,)), ((), ())),
+                preferred_element_type=jnp.float32,
+            )
+            spread = run_cols[rows, h : h + 1] - run_rows[h : h + 1, 0:wide]
+            here = b * 128 + lax.broadcasted_iota(jnp.int32, (128, wide), 0)
+            there = lax.broadcasted_iota(jnp.int32, (128, wide), 1)
+            table = jnp.exp(jnp.where(here >= there, spread, -jnp.inf))
+            inside[rows, vals] = jnp.dot(
+                (scores * table).astype(jnp.bfloat16), value_rows[pl.ds(0, wide), vals],
+                preferred_element_type=jnp.float32,
+            )
+
+
+def local_retention(queries, key_rows, value_rows, log_decay):
     length = queries.shape[0]
-    head_count = log_decay.shape[0]
-    key_width = queries.shape[1] // head_count
-    value_width = value_rows.shape[1] // head_count
-    blocks = length // BLOCK
-    positions = lax.axis_index("ep") * length + jnp.arange(length, dtype=jnp.int32)
-    query_rot = to_blocks(
-        rotate(queries.astype(jnp.float32).reshape(length, head_count, key_width), positions),
-        blocks,
-    )
-    key_rot = to_blocks(
-        rotate(key_rows.astype(jnp.float32).reshape(length, head_count, key_width), positions)
-        * key_width ** (-0.5),
-        blocks,
-    )
-    value_all = to_blocks(
-        value_rows.astype(jnp.float32).reshape(length, head_count, value_width), blocks
-    )
-    running = jnp.cumsum(log_decay.reshape(head_count, blocks, BLOCK), axis=2)
-    ending = running[:, :, -1]
-    kept = jnp.exp(ending[:, :, None] - running)
-    block_states = jnp.einsum("nlhd,hnl,nlhe->nhde", key_rot, kept, value_all)
-    block_decay = jnp.exp(ending).T
-
-    def advance(carried, inputs):
-        decay_now, state_now = inputs
-        return (decay_now[:, None, None] * carried + state_now, carried)
-
-    zeros_state = jnp.zeros((head_count, key_width, value_width), jnp.float32)
-    device_state, local_starts = lax.scan(advance, zeros_state, (block_decay, block_states))
-    device_decay = jnp.exp(jnp.sum(ending, axis=1))
-    incoming, passed_decay = prefix(
-        (device_state, device_decay),
-        "ep",
-        combine_states,
-        (zeros_state, jnp.ones((head_count,), jnp.float32)),
-    )
-    causal = jnp.arange(BLOCK)[:, None] >= jnp.arange(BLOCK)[None, :]
-    spread = running[:, :, :, None] - running[:, :, None, :]
-    weight_table = jnp.exp(jnp.where(causal, spread, -jnp.inf))
-    score_matrix = jnp.einsum("nlhd,nmhd->hnlm", query_rot, key_rot) * weight_table
-    inside = jnp.einsum("hnlm,nmhe->nlhe", score_matrix, value_all)
-    before = jnp.exp(jnp.cumsum(ending, axis=1) - ending)
-    starts = local_starts + before.T[:, :, None, None] * incoming[None]
-    outside = jnp.einsum("nlhd,hnl,nhde->nlhe", query_rot, jnp.exp(running), starts)
-    mixed = (inside + outside).reshape(length, head_count, value_width)
-    centered = mixed - jnp.mean(mixed, axis=-1, keepdims=True)
-    normed = (
-        centered
-        * lax.rsqrt(jnp.mean(centered * centered, axis=-1, keepdims=True) + epsilon)
-        * head_gain.reshape(head_count, value_width)
-    )
-    return (
-        jax.nn.silu(gate_rows.astype(jnp.float32))
-        * normed.reshape(length, head_count * value_width)
-    ).astype(jnp.bfloat16)
+    half = 64
+    positions = (lax.axis_index("ep") * length + jnp.arange(length, dtype=jnp.int32)).astype(jnp.float32)
+    frequency = theta_base ** (-jnp.arange(half, dtype=jnp.float32) / half)
+    angles = positions[:, None] * frequency
+    cosine, sine = jnp.cos(angles), jnp.sin(angles)
+    cosine = jnp.concatenate([cosine, cosine], axis=1)
+    sine = jnp.concatenate([-sine, sine], axis=1)
+    running = jnp.cumsum(log_decay, axis=1)
+    run_rows = jnp.pad(running, ((0, 4), (0, 0)))
+    run_cols = jnp.pad(running.T, ((0, 0), (0, 124)))
+    ending = jnp.broadcast_to(run_rows[:, -1:], (8, 256))
+    inside, scaled, state = pl.pallas_call(
+        local_kernel,
+        out_shape=(
+            jax.ShapeDtypeStruct((length, 1024), jnp.float32),
+            jax.ShapeDtypeStruct((length, 512), jnp.bfloat16),
+            jax.ShapeDtypeStruct((512, 256), jnp.float32),
+        ),
+        in_specs=[pl.BlockSpec(memory_space=pltpu.VMEM)] * 7,
+        out_specs=(pl.BlockSpec(memory_space=pltpu.VMEM),) * 3,
+        scratch_shapes=[pltpu.VMEM((length, 128), jnp.bfloat16), pltpu.VMEM((length, 128), jnp.bfloat16)],
+        compiler_params=pltpu.CompilerParams(vmem_limit_bytes=24 * 1024 * 1024),
+    )(queries, key_rows, value_rows, cosine, sine, run_cols, run_rows)
+    return inside, scaled, state, ending
 
 
 ROWS = 256
@@ -122,10 +76,13 @@
 MESH = pl.DeviceIdType.MESH
 
 
-def moe_kernel(
-    packed, meta, gate_w, up_w, down_w, mix_hi, mix_lo, out,
-    recv, meta_in, wg, wu, wd, inner, part, fwd_l, fwd_r, sum_r, sum_l, in_l, in_r, res, ret, acc,
-    d_send, d_recv, m_send, m_recv, own_sem, w_send, w_recv, w_own, x_send, x_recv, r_send, r_recv, r_own,
+def joint_kernel(
+    packed, meta, gate_w, up_w, down_w, mix_hi_h, mix_lo_h, out_w_h, gate_rows_h, inside, scaled, state, ending, gain,
+    out, mixer_out,
+    recv, meta_in, wg, wu, wd, inner, part, fwd_l, fwd_r, in_l, in_r, ret, acc, mix_hi, mix_lo, out_w, gate_rows,
+    hidden, half_out, half_in, half_end, ring, ring_end, edge_out, edge_in, incoming, b_fwd_l, b_fwd_r, b_in_l, b_in_r,
+    d_send, d_recv, m_send, m_recv, own_sem, w_send, w_recv, w_own, x_send, x_recv, r_send, r_recv, r_own, local_sem,
+    s_send, s_recv, s_own,
 ):
     ep, tp = lax.axis_index("ep"), lax.axis_index("tp")
     core, chip = ep % 2, ep // 2
@@ -147,6 +104,70 @@
     pl.semaphore_signal(barrier, inc=1, device_id=(chip * 2 + 1 - core, tp), device_id_type=MESH)
     pl.semaphore_wait(barrier, len(HOPS) + 3)
 
+    partner = (chip * 2 + 1 - core, tp)
+    locals_ = []
+    for i, (a, b) in enumerate(((mix_hi_h, mix_hi), (mix_lo_h, mix_lo), (out_w_h, out_w), (gate_rows_h, gate_rows))):
+        c = pltpu.make_async_copy(a, b, local_sem.at[i])
+        c.start()
+        locals_.append(c)
+
+    def state_copy(src, dst, i, to):
+        c = pltpu.make_async_remote_copy(
+            src_ref=src, dst_ref=dst, send_sem=s_send.at[i], recv_sem=s_recv.at[i],
+            device_id=to, device_id_type=MESH)
+        c.start()
+        return c
+
+    def heads_of(half):
+        return pl.ds(pl.multiple_of(half * 256, 256), 256)
+
+    def grown(value, ends, first):
+        return jnp.concatenate(
+            [value[:128] * jnp.exp(ends[first : first + 1]), value[128:] * jnp.exp(ends[first + 1 : first + 2])], axis=0
+        )
+
+    half_out[...] = state[heads_of(1 - core), :].astype(jnp.bfloat16)
+    swaps = [
+        state_copy(half_out, half_in, 0, partner),
+        state_copy(ending, half_end, 1, partner),
+    ]
+    for c in swaps:
+        c.wait_recv()
+    mine, other = state[heads_of(core), :], half_in[...].astype(jnp.float32)
+    own_end = jnp.where(core == 0, ending[0:2, :], ending[2:4, :])
+    other_end = jnp.where(core == 0, half_end[0:2, :], half_end[2:4, :])
+    before, after = jnp.where(core == 0, mine, other), jnp.where(core == 0, other, mine)
+    before_end, after_end = jnp.where(core == 0, own_end, other_end), jnp.where(core == 0, other_end, own_end)
+
+    def level(base, value, ends, place, sem, peers):
+        ring[base + 4] = value.astype(jnp.bfloat16)
+        ring_end[base + 4] = jnp.concatenate([ends, jnp.zeros((6, 256), jnp.float32)], axis=0)
+        copies = []
+        for d in (1, 3, 2):
+            copies.append(state_copy(ring.at[base + 4], ring.at[base + place], sem + 2 * d, peers(d)))
+            copies.append(state_copy(ring_end.at[base + 4], ring_end.at[base + place], sem + 2 * d + 1, peers(d)))
+        return copies
+
+    def collect(base, value, ends, place, copies):
+        for c in copies:
+            c.wait_recv()
+        ring[base + place] = value.astype(jnp.bfloat16)
+        ring_end[base + place] = jnp.concatenate([ends, jnp.zeros((6, 256), jnp.float32)], axis=0)
+        prefix, total = jnp.zeros((256, 256), jnp.float32), jnp.zeros((256, 256), jnp.float32)
+        prefix_end, total_end = jnp.zeros((2, 256), jnp.float32), jnp.zeros((2, 256), jnp.float32)
+        for j in range(4):
+            e, v = ring_end[base + j, 0:2, :], ring[base + j].astype(jnp.float32)
+            prefix = jnp.where(j < place, grown(prefix, e, 0) + v, prefix)
+            prefix_end = jnp.where(j < place, prefix_end + e, prefix_end)
+            total = grown(total, e, 0) + v
+            total_end = total_end + e
+        return prefix, prefix_end, total, total_end
+
+    chip_state = grown(before, after_end, 0) + after
+    chip_end = before_end + after_end
+    row_copies = level(0, chip_state, chip_end, y, 0, lambda d: ((z * 4 + (y + d) % 4) * 2 + core, tp))
+    row_prefix, row_prefix_end, row_state, row_end = collect(0, chip_state, chip_end, y, row_copies)
+    plane_copies = level(5, row_state, row_end, z, 8, lambda d: ((((z + d) % 4) * 4 + y) * 2 + core, tp))
     metas, sends = [], []
     for i, (dz, dy) in enumerate(HOPS):
         t = chip_at(dz, dy)
@@ -184,6 +205,14 @@
     c = pltpu.make_async_copy(meta.at[rows_of(chip)], meta_in.at[rows_of(chip)], own_sem.at[CHUNKS])
     c.start()
     owns.append(c)
+    plane_prefix, _, _, _ = collect(5, row_state, row_end, z, plane_copies)
+    chip_prefix = grown(plane_prefix, row_prefix_end, 0) + row_prefix
+    core_prefix = grown(chip_prefix, before_end, 0) + before
+    edge_out[...] = jnp.where(core == 0, core_prefix, chip_prefix).astype(jnp.bfloat16)
+    edge = state_copy(edge_out, edge_in, 16, partner)
+    incoming[heads_of(core), :] = jnp.where(core == 0, chip_prefix, core_prefix).astype(jnp.bfloat16)
+    edge.wait_recv()
+    incoming[heads_of(1 - core), :] = edge_in[...]
 
     def x_copy(src, dst, slot, k, to):
         return pltpu.make_async_remote_copy(
@@ -238,27 +267,27 @@
 
     def forward(k):
         xs[k, 0].wait_recv()
-        sum_r[k] = (fwd_l[k].astype(jnp.float32) + part[k, right, top].astype(jnp.float32)).astype(jnp.bfloat16)
-        xs[k, 4] = launch(x_copy(sum_r.at[k], in_l.at[k, top], 4, k, right))
+        fwd_l[k] = (fwd_l[k].astype(jnp.float32) + part[k, right, top].astype(jnp.float32)).astype(jnp.bfloat16)
+        xs[k, 4] = launch(x_copy(fwd_l.at[k], in_l.at[k, top], 4, k, right))
         xs[k, 1].wait_recv()
-        sum_l[k] = (fwd_r[k].astype(jnp.float32) + part[k, left, low].astype(jnp.float32)).astype(jnp.bfloat16)
-        xs[k, 5] = launch(x_copy(sum_l.at[k], in_r.at[k, low], 5, k, left))
+        fwd_r[k] = (fwd_r[k].astype(jnp.float32) + part[k, left, low].astype(jnp.float32)).astype(jnp.bfloat16)
+        xs[k, 5] = launch(x_copy(fwd_r.at[k], in_r.at[k, low], 5, k, left))
 
     def finish(k):
         for s in (2, 3, 4, 5):
             xs[k, s].wait_recv()
-        res[k] = (
+        in_l[k] = (
             part[k, tp].astype(jnp.float32) + in_l[k].astype(jnp.float32) + in_r[k].astype(jnp.float32)
         ).astype(jnp.bfloat16)
         row = []
         for i, (dz, dy) in enumerate(HOPS):
             t = chip_at(dz, dy)
             c = pltpu.make_async_remote_copy(
-                src_ref=res.at[k, rows_of(t)], dst_ref=ret.at[k, rows_of(chip)],
+                src_ref=in_l.at[k, rows_of(t)], dst_ref=ret.at[k, rows_of(chip)],
                 send_sem=r_send.at[k, i], recv_sem=r_recv.at[k, i],
                 device_id=(t * 2 + core, tp), device_id_type=MESH)
             row.append(launch(c))
-        mine = pltpu.make_async_copy(res.at[k, rows_of(chip)], ret.at[k, rows_of(chip)], r_own.at[k])
+        mine = pltpu.make_async_copy(in_l.at[k, rows_of(chip)], ret.at[k, rows_of(chip)], r_own.at[k])
         mine.start()
         returns[k] = (row, mine)
 
@@ -279,6 +308,73 @@
             else:
                 out[:, f] = (acc[:, f] + part_sum).astype(jnp.bfloat16)
 
+    def head_rows(b, carry):
+        rows = pl.ds(pl.multiple_of(b * 128, 128), 128)
+        for h in range(4):
+            vals = pl.ds(h * 256, 256)
+            o = inside[rows, vals] + jnp.dot(
+                scaled[rows, pl.ds(h * 128, 128)], incoming[pl.ds(h * 128, 128), :], preferred_element_type=jnp.float32
+            )
+            o = o - jnp.mean(o, axis=-1, keepdims=True)
+            o = o * lax.rsqrt(jnp.mean(o * o, axis=-1, keepdims=True) + epsilon) * gain[0:1, vals]
+            g = gate_rows[rows, vals].astype(jnp.float32)
+            hidden[rows, vals] = (g / (1.0 + jnp.exp(-g)) * o).astype(jnp.bfloat16)
+        return carry
+
+    btop, blow = pl.ds(0, 64), pl.ds(64, 64)
+    mixer_sends = []
+
+    def block_part(n, q, lower, count):
+        return part.at[2 + n // 2, q, pl.ds((n % 2) * 128 + lower, count)]
+
+    def project(n):
+        def strip(i, carry):
+            cols = pl.ds(pl.multiple_of(n * QUARTER + i * 256, 256), 256)
+            total = jnp.dot(hidden[...], out_w[:, cols], preferred_element_type=jnp.float32).astype(jnp.bfloat16)
+            for q in range(4):
+                part[2 + n // 2, q, pl.ds((n % 2) * 128, 128), pl.ds(pl.multiple_of(i * 256, 256), 256)] = total[
+                    q * 128 : (q + 1) * 128
+                ]
+            return carry
+
+        lax.fori_loop(0, 4, strip, 0)
+        k = CHUNKS + n
+        xs[k, 0] = x_copy(block_part(n, far, 0, 64), b_fwd_l.at[n], 0, k, right)
+        xs[k, 1] = x_copy(block_part(n, far, 64, 64), b_fwd_r.at[n], 1, k, left)
+        xs[k, 2] = x_copy(block_part(n, right, 64, 64), b_in_l.at[n, blow], 2, k, right)
+        xs[k, 3] = x_copy(block_part(n, left, 0, 64), b_in_r.at[n, btop], 3, k, left)
+        for i in range(4):
+            xs[k, i].start()
+            mixer_sends.append(xs[k, i])
+
+    def pass_on(n):
+        k = CHUNKS + n
+        for slot, buf, own, dst, to in (
+            (0, b_fwd_l, block_part(n, right, 0, 64), b_in_l.at[n, btop], right),
+            (1, b_fwd_r, block_part(n, left, 64, 64), b_in_r.at[n, blow], left),
+        ):
+            xs[k, slot].wait_recv()
+            buf[n] = (buf[n].astype(jnp.float32) + own[...].astype(jnp.float32)).astype(jnp.bfloat16)
+            xs[k, 4 + slot] = launch(x_copy(buf.at[n], dst, 4 + slot, k, to))
+
+    def close(n):
+        k = CHUNKS + n
+        for i in (2, 3, 4, 5):
+            xs[k, i].wait_recv()
+        mixer_out[:, pl.ds(n * QUARTER, QUARTER)] = (
+            block_part(n, tp, 0, 128)[...].astype(jnp.float32)
+            + b_in_l[n].astype(jnp.float32)
+            + b_in_r[n].astype(jnp.float32)
+        ).astype(jnp.bfloat16)
+
+    for c in locals_:
+        c.wait()
+    lax.fori_loop(0, 4, head_rows, 0)
+    for n in range(4):
+        project(n)
+        if n > 0:
+            pass_on(n - 1)
+    pass_on(3)
     for c, own in weights:
         own.wait()
         c.wait_recv()
@@ -289,6 +385,11 @@
         for c in sends[k]:
             c.wait_recv()
         owns[k].wait()
+        if k == 2:
+            for n in range(4):
+                close(n)
+            for c in mixer_sends:
+                c.wait_send()
         compute(k)
         if k > 0:
             finish(k - 1)
@@ -300,7 +401,7 @@
     combine(CHUNKS - 1)
     for c, own in weights:
         c.wait_send()
-    for c in metas:
+    for c in metas + swaps + row_copies + plane_copies + [edge]:
         c.wait_send()
     for row in sends:
         for c in row:
@@ -315,7 +416,7 @@
 )
 
 
-def routed(normed, route_ids, route_weight, gate_w, up_w, down_w):
+def joint(normed, route_ids, route_weight, gate_w, up_w, down_w, out_w, gate_rows, inside, scaled, state, ending, gain):
     tokens, width = normed.shape
     experts = 32
     kinds = jnp.arange(experts, dtype=jnp.int32)
@@ -343,10 +444,13 @@
     bf = jnp.bfloat16
     dma = pltpu.SemaphoreType.DMA
     return pl.pallas_call(
-        moe_kernel,
-        out_shape=jax.ShapeDtypeStruct((tokens, QUARTER), bf),
-        in_specs=[any_space, any_space, any_space, any_space, any_space, vmem, vmem],
-        out_specs=vmem,
+        joint_kernel,
+        out_shape=(
+            jax.ShapeDtypeStruct((tokens, QUARTER), bf),
+            jax.ShapeDtypeStruct((tokens // 4, width), bf),
+        ),
+        in_specs=[any_space] * 9 + [vmem] * 5,
+        out_specs=(vmem, vmem),
         scratch_shapes=[
             pltpu.VMEM((CHUNKS, ROWS, width), bf),
             pltpu.VMEM((256, 128), bf),
@@ -357,21 +461,38 @@
             pltpu.VMEM((CHUNKS, 4, ROWS, QUARTER), bf),
             pltpu.VMEM((CHUNKS, 128, QUARTER), bf),
             pltpu.VMEM((CHUNKS, 128, QUARTER), bf),
-            pltpu.VMEM((CHUNKS, 128, QUARTER), bf),
-            pltpu.VMEM((CHUNKS, 128, QUARTER), bf),
-            pltpu.VMEM((CHUNKS, ROWS, QUARTER), bf),
             pltpu.VMEM((CHUNKS, ROWS, QUARTER), bf),
             pltpu.VMEM((CHUNKS, ROWS, QUARTER), bf),
             pltpu.VMEM((CHUNKS, ROWS, QUARTER), bf),
             pltpu.VMEM((tokens, QUARTER), jnp.float32),
+            pltpu.VMEM((tokens, QUARTER), bf),
+            pltpu.VMEM((tokens, QUARTER), bf),
+            pltpu.VMEM((1024, width), bf),
+            pltpu.VMEM((tokens, 1024), bf),
+            pltpu.VMEM((tokens, 1024), bf),
+            pltpu.VMEM((256, 256), bf),
+            pltpu.VMEM((256, 256), bf),
+            pltpu.VMEM((8, 256), jnp.float32),
+            pltpu.VMEM((10, 256, 256), bf),
+            pltpu.VMEM((10, 8, 256), jnp.float32),
+            pltpu.VMEM((256, 256), bf),
+            pltpu.VMEM((256, 256), bf),
+            pltpu.VMEM((512, 256), bf),
+            pltpu.VMEM((4, 64, QUARTER), bf),
+            pltpu.VMEM((4, 64, QUARTER), bf),
+            pltpu.VMEM((4, 128, QUARTER), bf),
+            pltpu.VMEM((4, 128, QUARTER), bf),
             dma((CHUNKS, 15)), dma((CHUNKS, 15)), dma((15,)), dma((15,)), dma((CHUNKS + 1,)),
-            dma((3,)), dma((3,)), dma((3,)), dma((6, CHUNKS)), dma((6, CHUNKS)),
-            dma((CHUNKS, 15)), dma((CHUNKS, 15)), dma((CHUNKS,)),
+            dma((3,)), dma((3,)), dma((3,)), dma((6, CHUNKS + 4)), dma((6, CHUNKS + 4)),
+            dma((CHUNKS, 15)), dma((CHUNKS, 15)), dma((CHUNKS,)), dma((4,)), dma((17,)), dma((17,)), dma((1,)),
         ],
         compiler_params=pltpu.CompilerParams(
-            collective_id=0, has_side_effects=True, vmem_limit_bytes=60 * 1024 * 1024
+            collective_id=0, has_side_effects=True, vmem_limit_bytes=67043328
         ),
-    )(packed.reshape(CHUNKS, ROWS, width), meta, gate_w[0], up_w[0], down_w[0], mix_hi, mix_lo)
+    )(
+        packed.reshape(CHUNKS, ROWS, width), meta, gate_w[0], up_w[0], down_w[0], mix_hi, mix_lo, out_w, gate_rows,
+        inside, scaled, state, ending, gain.reshape(1, 1024),
+    )
 
 
 def body(
@@ -390,20 +511,17 @@
     expert_up,
     expert_down,
 ):
-    hidden = retention_rows(queries, key_rows, value_rows, gate_rows, log_decay, head_gain)
-    mixer_out = lax.psum_scatter(
-        jnp.dot(hidden, out_weight, preferred_element_type=jnp.float32).astype(jnp.bfloat16),
-        "tp",
-        scatter_dimension=0,
-        tiled=True,
-    )
+    inside, scaled, state, ending = local_retention(queries, key_rows, value_rows, log_decay)
     widened = expert_input.astype(jnp.float32)
     normed = (
         widened
         * lax.rsqrt(jnp.mean(widened * widened, axis=-1, keepdims=True) + epsilon)
         * input_gain
     ).astype(jnp.bfloat16)
-    expert_out = routed(normed, route_ids, route_weight, expert_gate, expert_up, expert_down)
+    expert_out, mixer_out = joint(
+        normed, route_ids, route_weight, expert_gate, expert_up, expert_down, out_weight, gate_rows,
+        inside, scaled, state, ending, head_gain,
+    )
     return (mixer_out, expert_out)
 
 

time: 337 us -> 194 us (0.58)
  blocking collectives: 69.8 us -> 0 us
  other arithmetic: 48.4 us -> 8.66 us
  matrix products: 30.7 us -> 7.43 us
  Pallas kernels: 150 us -> 169 us
  between operations: 14.9 us -> 0.86 us
  local copies, waits for them, and re-layouts: 21.3 us -> 7.94 us
    unnamed x1 -> x0, blocking collectives: 69.8 us -> none
    select_n x32 -> x0, other arithmetic: 34.9 us -> none  [hop(): return jax.tree.map(lambda a, b: jnp.where(reached, a, b), new, before)]
    dot_general x6 -> x2, matrix products: 30.7 us -> 7.43 us  [the longest x1 7.13 us: joint(): jnp.dot(chosen.astype(jnp.bfloat16), normed, preferred_element_type=jnp.f...]
    pallas_call x1 -> x2, Pallas kernels: 150 us -> 169 us  [the longest x1 166 us: joint(): pl.pallas_call(joint_kernel, out_shape=(jax.ShapeDtypeStruct((tokens, QUA...]
    unnamed x27 -> x28, local copies, waits for them, and re-layouts: 12.4 us -> 6.61 us
    sub x2 -> x0, local copies, waits for them, and re-layouts: 4.48 us -> none  [retention_rows(): centered = mixed - jnp.mean(mixed, axis=-1, keepdims=True)]
    sub x1 -> x0, other arithmetic: 4.13 us -> none  [rotate(): first_half * cosine - second * sine_wave]
  transfers between devices with their start and end apart: 2 -> 0, of which waited for: 0 -> 0; matrix products, arithmetic and copies ran while one was open for 6% -> 0% of each run, Pallas kernels for 45% -> 0%
where the time goes in v2:
time: 194 us
  Pallas kernels  169 us (87%)
  other arithmetic  8.66 us (4%)
  local copies, waits for them, and re-layouts  7.94 us (4%)
  matrix products  7.43 us (4%)
    pallas_call x1, Pallas kernels, joint(): pl.pallas_call(joint_kernel, out_shape=(jax.ShapeDtypeStruct((tokens, QUA...  166 us
    dot_general x1, matrix products, joint(): jnp.dot(chosen.astype(jnp.bfloat16), normed, preferred_element_type=jnp.f...  7.13 us
    unnamed x28, local copies, waits for them, and re-layouts  6.61 us

profile of v2, /device:TPU:0, one launch (start us, length us, event | category | flops | bytes accessed | tf_op | source)
XLA Modules:
  0.0 193.5 jit_solution(3809000581047392040)
XLA Ops:
  0.7 0.0 copy-start.10
  0.7 0.0 copy-start.9
  0.7 0.0 copy-start.8
  0.7 3.1 %fusion = f32[512]{0:T(512)S(1)} fusion(bf16[512,4096]{1,0:T(8,128)(2,1)} %param.21), kind=kLoop, calls=%fused_computation.2 | loop fusion | flops 6290944 | bytes 4196352 | tf_op jit(solution)/shard_map/reduce_sum | solution.py:518
  3.8 0.0 copy-done.10
  3.9 0.0 copy-done.9
  3.9 1.2 reduce-window.6
  5.1 0.2 slice_reduce_fusion
  5.3 0.2 reduce-window.9
  5.5 0.1 add_bitcast_fusion
  5.5 0.2 slice_reduce_fusion.1
  5.7 0.7 broadcast_in_dim.71.ending
  6.4 0.0 copy-done.8
  6.4 0.1 convert_reduce_fusion
  6.5 0.1 slice.28
  6.7 0.1 lt.36
  6.7 0.1 lt.37
  6.8 0.3 fusion.16
  7.2 0.7 fusion.12.meta
  7.9 0.1 copy.23
  8.1 0.0 copy-start.1
  8.1 0.0 copy-start.4
  8.1 0.0 copy-start.5
  8.1 1.0 fusion.13
  9.1 0.2 pad_maximum_fusion
  9.3 0.0 copy-start.6
  9.3 0.0 copy-start.11
  9.3 2.0 %fusion.6 = (bf16[512,1024]{1,0:T(8,128)(2,1)}, bf16[512,1024]{1,0:T(8,128)(2,1)}) fusion(f32[512]{0:T(512)S(1)} %bitcast.33, s32[512]{0:T(512)S(1)} %bitcast.36, f32[512]{0:T(512)S(1)} %bitcast.32, s32[512]{0:T(512)S(1)} %bitcast.34), kind=kLoop, calls=%fused_computation.10 | loop fusion | flops 4718592 | bytes 2105344 | tf_op jit(solution)/shard_map/convert_element_type | solution.py:439
  11.3 0.0 copy-done.1
  11.3 0.0 copy-done.4
  11.3 0.0 copy-done.5
  11.3 2.6 %shard_map.149 = (f32[512,1024]{1,0:T(8,128)S(1)}, bf16[512,512]{1,0:T(8,128)(2,1)S(1)}, f32[512,256]{1,0:T(8,128)S(1)}) custom-call(bf16[512,512]{1,0:T(8,128)(2,1)S(1)} %copy-done.4, bf16[512,512]{1,0:T(8,128)(2,1)S(1)} %copy-done.5, bf16[512,1024]{1,0:T(8,128)(2,1)S(1)} %copy-done.1, f32[512,128]{1,0:T(8,128)S(1)} %get-tuple-element.23.cosine, ...), custom_call_target="tpu_custom_call" | custom-call | tf_op jit(solution)/shard_map/pallas_call | solution.py:58
  13.9 0.0 copy-start
  13.9 1.4 copy-done
  15.3 0.0 copy-start.2
  15.3 0.8 copy-done.2
  16.1 0.0 copy-start.3
  16.1 0.8 copy-done.3
  17.0 0.0 copy-done.6
  17.0 0.0 copy-done.11
  17.0 7.1 %convolution_convert_fusion = bf16[1024,4096]{1,0:T(8,128)(2,1)} fusion(bf16[512,4096]{1,0:T(8,128)(2,1)S(1)} %copy-done.6, f32[4096]{0:T(1024)S(1)} %copy-done.11, f32[512]{0:T(512)S(1)} %add_rsqrt_fusion, s32[512]{0:T(512)S(1)} %bitcast.37, s32[512]{0:T(512)S(1)} %bitcast.35), kind=kOutput, calls=%fused_computation.5 | convolution fusion | flops 4309123072 | bytes 12605440 | tf_op jit(solution)/shard_map/dot_general | solution.py:433
  24.1 166.1 %shard_map.150 = (bf16[512,1024]{1,0:T(8,128)(2,1)}, bf16[128,4096]{1,0:T(8,128)(2,1)}) custom-call(bf16[4,256,4096]{2,1,0:T(8,128)(2,1)} %bitcast.24, bf16[256,128]{1,0:T(8,128)(2,1)} %fusion.12.meta, bf16[4096,256]{1,0:T(8,128)(2,1)} %bitcast.25, bf16[4096,256]{1,0:T(8,128)(2,1)} %bitcast.26, bf16[256,4096]{1,0:T(8,128)(2,1)} %bitcast.27, ...), custom_call_target="tpu_custom_call" | custom-call | tf_op jit(solution)/shard_map/pallas_call | solution.py:446
  190.2 0.0 copy-start.7
  190.2 2.4 %copy.31 = bf16[128,4096]{1,0:T(8,128)(2,1)} copy(bf16[128,4096]{1,0:T(8,128)(2,1)} %get-tuple-element.27) | data formatting | bytes 2097152
  192.6 0.0 copy-done.7
  192.6 1.0 copy.32
  (16 shorter events, 0.2 us)
Async XLA Ops:
  0.7 3.1 %copy-start.10 = (f32[512,2]{0,1:T(2,128)S(1)}, f32[512,2]{0,1:T(2,128)}, u32[]{:S(2)}) copy-start(f32[512,2]{0,1:T(2,128)} %param.24) | copy-start | bytes 12292
  0.7 3.2 %copy-start.9 = (f32[4,512]{1,0:T(4,128)S(1)}, f32[4,512]{1,0:T(4,128)}, u32[]{:S(2)}) copy-start(f32[4,512]{1,0:T(4,128)} %param.18) | copy-start | bytes 24580
  0.7 5.7 %copy-start.8 = (s32[512,2]{0,1:T(2,128)S(1)}, s32[512,2]{0,1:T(2,128)}, u32[]{:S(2)}) copy-start(s32[512,2]{0,1:T(2,128)} %param.23) | copy-start | bytes 12292
  8.1 3.2 %copy-start.1 = (bf16[512,1024]{1,0:T(8,128)(2,1)S(1)}, bf16[512,1024]{1,0:T(8,128)(2,1)}, u32[]{:S(2)}) copy-start(bf16[512,1024]{1,0:T(8,128)(2,1)} %value_rows.1) | copy-start | bytes 3145732
  8.1 3.2 %copy-start.4 = (bf16[512,512]{1,0:T(8,128)(2,1)S(1)}, bf16[512,512]{1,0:T(8,128)(2,1)}, u32[]{:S(2)}) copy-start(bf16[512,512]{1,0:T(8,128)(2,1)} %queries.1) | copy-start | bytes 1572868
  8.1 3.2 %copy-start.5 = (bf16[512,512]{1,0:T(8,128)(2,1)S(1)}, bf16[512,512]{1,0:T(8,128)(2,1)}, u32[]{:S(2)}) copy-start(bf16[512,512]{1,0:T(8,128)(2,1)} %key_rows.1) | copy-start | bytes 1572868
  9.3 7.6 %copy-start.6 = (bf16[512,4096]{1,0:T(8,128)(2,1)S(1)}, bf16[512,4096]{1,0:T(8,128)(2,1)}, u32[]{:S(2)}) copy-start(bf16[512,4096]{1,0:T(8,128)(2,1)} %param.21) | copy-start | bytes 12582916
  9.3 7.6 %copy-start.11 = (f32[4096]{0:T(1024)S(1)}, f32[4096]{0:T(1024)}, u32[]{:S(2)}) copy-start(f32[4096]{0:T(1024)} %param.22) | copy-start | bytes 49156
  13.9 1.4 copy-start
  15.3 0.8 copy-start.2
  16.1 0.8 copy-start.3
  190.2 2.4 %copy-start.7 = (bf16[512,1024]{1,0:T(8,128)(2,1)S(1)}, bf16[512,1024]{1,0:T(8,128)(2,1)}, u32[]{:S(2)}) copy-start(bf16[512,1024]{1,0:T(8,128)(2,1)} %get-tuple-element.28) | copy-start | bytes 3145732

commit v3 on v2

v3 whole, which is shorter than its diff:
```python
import jax
import jax.numpy as jnp
from jax import lax
from jax.experimental import pallas as pl
from jax.experimental.pallas import tpu as pltpu
from jax.sharding import PartitionSpec as P


epsilon = 1e-06
theta_base = 10000.0

def local_kernel(queries, key_rows, value_rows, cosine, sine, run_cols, run_rows, inside, scaled, state, keys, mixed_q):
    half = 64
    for h in range(4):
        cols, vals = pl.ds(h * 128, 128), pl.ds(h * 256, 256)
        q = queries[:, cols].astype(jnp.float32)
        k = key_rows[:, cols].astype(jnp.float32)
        q = q * cosine[...] + pltpu.roll(q, half, 1) * sine[...]
        k = (k * cosine[...] + pltpu.roll(k, half, 1) * sine[...]) * 128.0 ** (-0.5)
        run = run_cols[:, h : h + 1]
        ending = run_rows[h : h + 1, 511:512]
        keys[...] = k.astype(jnp.bfloat16)
        mixed_q[...] = q.astype(jnp.bfloat16)
        scaled[:, cols] = (q * jnp.exp(run)).astype(jnp.bfloat16)
        kept = (k * jnp.exp(ending - run)).astype(jnp.bfloat16)
        state[pl.ds(h * 128, 128), :] = lax.dot_general(
            kept, value_rows[:, vals], (((0,), (0,)), ((), ())), preferred_element_type=jnp.float32
        ).astype(jnp.bfloat16)
        for b in range(4):
            rows, wide = pl.ds(b * 128, 128), (b + 1) * 128
            scores = lax.dot_general(
                mixed_q[rows, :], keys[pl.ds(0, wide), :], (((1,), (1,)), ((), ())),
                preferred_element_type=jnp.float32,
            )
            spread = run_cols[rows, h : h + 1] - run_rows[h : h + 1, 0:wide]
            here = b * 128 + lax.broadcasted_iota(jnp.int32, (128, wide), 0)
            there = lax.broadcasted_iota(jnp.int32, (128, wide), 1)
            table = jnp.exp(jnp.where(here >= there, spread, -jnp.inf))
            inside[rows, vals] = jnp.dot(
                (scores * table).astype(jnp.bfloat16), value_rows[pl.ds(0, wide), vals],
                preferred_element_type=jnp.float32,
            )


def local_retention(queries, key_rows, value_rows, log_decay):
    length = queries.shape[0]
    half = 64
    positions = (lax.axis_index("ep") * length + jnp.arange(length, dtype=jnp.int32)).astype(jnp.float32)
    frequency = theta_base ** (-jnp.arange(half, dtype=jnp.float32) / half)
    angles = positions[:, None] * frequency
    cosine, sine = jnp.cos(angles), jnp.sin(angles)
    cosine = jnp.concatenate([cosine, cosine], axis=1)
    sine = jnp.concatenate([-sine, sine], axis=1)
    running = jnp.cumsum(log_decay, axis=1)
    run_rows = jnp.pad(running, ((0, 4), (0, 0)))
    run_cols = jnp.pad(running.T, ((0, 0), (0, 124)))
    ending = jnp.broadcast_to(run_rows[:, -1:], (8, 256))
    inside, scaled, state = pl.pallas_call(
        local_kernel,
        out_shape=(
            jax.ShapeDtypeStruct((length, 1024), jnp.float32),
            jax.ShapeDtypeStruct((length, 512), jnp.bfloat16),
            jax.ShapeDtypeStruct((512, 256), jnp.bfloat16),
        ),
        in_specs=[pl.BlockSpec(memory_space=pltpu.VMEM)] * 7,
        out_specs=(pl.BlockSpec(memory_space=pltpu.VMEM),) * 3,
        scratch_shapes=[pltpu.VMEM((length, 128), jnp.bfloat16), pltpu.VMEM((length, 128), jnp.bfloat16)],
        compiler_params=pltpu.CompilerParams(vmem_limit_bytes=24 * 1024 * 1024),
    )(queries, key_rows, value_rows, cosine, sine, run_cols, run_rows)
    return inside, scaled, state, ending


ROWS = 256
CHUNKS = 4
QUARTER = 1024
MESH = pl.DeviceIdType.MESH


def joint_kernel(
    rows_h, row_gain, spot_rows, spot_cols, weight_cols, meta, gate_w, up_w, down_w, out_w_h, gate_rows_h, inside_h,
    scaled, state, ending, gain,
    out, mixer_out,
    recv, meta_in, wg, wu, wd, inner, part, mixed, fwd_l, fwd_r, in_l, in_r, ret, acc, out_w, gate_rows,
    hidden, gathered, gathered_end, before, total_out, total_end, plane, plane_end, starts, incoming, b_fwd_l, b_fwd_r, b_in_l, b_in_r,
    d_send, d_recv, m_send, m_recv, own_sem, w_send, w_recv, w_own, x_send, x_recv, r_send, r_recv, r_own, local_sem,
    s_send, s_recv,
):
    ep, tp = lax.axis_index("ep"), lax.axis_index("tp")
    core, chip = ep % 2, ep // 2
    z, y = chip // 4, chip % 4
    right, left = (tp + 1) % 4, (tp + 3) % 4
    far = (tp + 2) % 4

    def chip_at(dz, dy):
        return ((z + dz) % 4) * 4 + (y + dy) % 4

    def rows_of(c):
        return pl.ds(pl.multiple_of(c * 16, 16), 16)

    def spot_of(i):
        return pl.ds((i if i < OWN else i + 1) * 16, 16)

    barrier = pltpu.get_barrier_semaphore()
    for dz, dy in HOPS:
        pl.semaphore_signal(barrier, inc=1, device_id=(chip_at(dz, dy) * 2 + core, tp), device_id_type=MESH)
    for t in (left, right):
        pl.semaphore_signal(barrier, inc=1, device_id=(ep, t), device_id_type=MESH)
    for d in range(4):
        t = (z * 4 + (y + d) % 4) * 2 + 1 - core
        pl.semaphore_signal(barrier, inc=1, device_id=(t, tp), device_id_type=MESH)

    partner = (chip * 2 + 1 - core, tp)
    normed = out_w.at[pl.ds(0, 512)]
    rows_in = pltpu.make_async_copy(rows_h, normed, local_sem.at[0])
    rows_in.start()
    locals_ = []
    for i, (a, b) in enumerate(((inside_h, acc), (gate_rows_h, gate_rows))):
        c = pltpu.make_async_copy(a, b, local_sem.at[1 + i])
        c.start()
        locals_.append(c)

    def state_copy(src, dst, i, to):
        c = pltpu.make_async_remote_copy(
            src_ref=src, dst_ref=dst, send_sem=s_send.at[i], recv_sem=s_recv.at[i],
            device_id=to, device_id_type=MESH)
        c.start()
        return c

    rows_in.wait()

    def norm_rows(b, carry):
        rows = pl.ds(pl.multiple_of(b * 16, 16), 16)
        v = out_w[rows, :].astype(jnp.float32)
        scale = lax.rsqrt(jnp.mean(v * v, axis=-1, keepdims=True) + epsilon)
        out_w[rows, :] = (v * scale * row_gain[...]).astype(jnp.bfloat16)
        return carry

    lax.fori_loop(0, 32, norm_rows, 0)

    def pack(k):
        entry = k * ROWS + lax.broadcasted_iota(jnp.int32, (ROWS, 512), 0)
        chosen = jnp.where((entry == spot_rows[0:1, :]) | (entry == spot_rows[1:2, :]), 1.0, 0.0).astype(jnp.bfloat16)

        def strip(i, carry):
            cols = pl.ds(pl.multiple_of(i * 512, 512), 512)
            part[k, i // 2, :, pl.ds(pl.multiple_of((i % 2) * 512, 512), 512)] = jnp.dot(
                chosen, out_w[pl.ds(0, 512), cols], preferred_element_type=jnp.float32
            ).astype(jnp.bfloat16)
            return carry

        lax.fori_loop(0, 8, strip, 0)

    sends, owns = {}, {}

    def dispatch(k, hops):
        for i in hops:
            t = chip_at(*HOPS[i])
            c = pltpu.make_async_remote_copy(
                src_ref=part.at[k, :, rows_of(t)], dst_ref=recv.at[k, :, spot_of(i)],
                send_sem=d_send.at[k, i], recv_sem=d_recv.at[k, i],
                device_id=(t * 2 + core, tp), device_id_type=MESH)
            c.start()
            sends[k, i] = c

    def keep(k):
        owns[k] = pltpu.make_async_copy(part.at[k, :, rows_of(chip)], recv.at[k, :, pl.ds(OWN * 16, 16)], own_sem.at[k])
        owns[k].start()

    pl.semaphore_wait(barrier, len(HOPS) + 6)
    place = y * 2 + core
    head = place // 2

    def slice_of(p):
        return pl.ds(pl.multiple_of(p * 64, 64), 64)

    def row_peer(dy, dc):
        return (y + dy) % 4, (core + dc) % 2

    spreads = []
    for i, hop in enumerate(ROW_HOPS):
        py, pc = row_peer(*hop)
        to = ((z * 4 + py) * 2 + pc, tp)
        spreads.append(state_copy(state.at[slice_of(py * 2 + pc)], gathered.at[place], i, to))
        spreads.append(state_copy(ending, gathered_end.at[place], 7 + i, to))
    pack(0)
    gathered[place] = state[slice_of(place), :]
    gathered_end[place] = ending[...]
    for c in spreads:
        c.wait_recv()
    carried, reach = jnp.zeros((64, 256), jnp.float32), jnp.zeros((1, 256), jnp.float32)
    reaches = []
    for k in range(8):
        e = gathered_end[k, pl.ds(head, 1), :]
        before[k] = carried
        reaches.append(reach)
        carried = carried * jnp.exp(e) + gathered[k].astype(jnp.float32)
        reach = reach + e
    total_out[...] = carried.astype(jnp.bfloat16)
    total_end[...] = jnp.broadcast_to(reach, (8, 256))
    planes = []
    for d in (1, 3, 2):
        to = ((((z + d) % 4) * 4 + y) * 2 + core, tp)
        planes.append(state_copy(total_out, plane.at[z], 12 + 2 * d, to))
        planes.append(state_copy(total_end, plane_end.at[z], 13 + 2 * d, to))
    pack(1)
    plane[z] = carried.astype(jnp.bfloat16)
    plane_end[z] = jnp.broadcast_to(reach, (8, 256))
    for c in planes:
        c.wait_recv()
    carried = jnp.zeros((64, 256), jnp.float32)
    for k in range(4):
        later = carried * jnp.exp(plane_end[k, 0:1, :]) + plane[k].astype(jnp.float32)
        carried = jnp.where(k < z, later, carried)
    for k in range(8):
        starts[k] = (carried * jnp.exp(reaches[k]) + before[k]).astype(jnp.bfloat16)
    edges = []
    for i, hop in enumerate(ROW_HOPS):
        py, pc = row_peer(*hop)
        to = ((z * 4 + py) * 2 + pc, tp)
        edges.append(state_copy(starts.at[py * 2 + pc], incoming.at[slice_of(place)], 20 + i, to))
    incoming[slice_of(place), :] = starts[place]
    dispatch(0, FAR + NEAR)
    keep(0)
    metas = []
    for i, hop in enumerate(HOPS):
        t = chip_at(*hop)
        c = pltpu.make_async_remote_copy(
            src_ref=meta.at[rows_of(t)], dst_ref=meta_in.at[spot_of(i)],
            send_sem=m_send.at[i], recv_sem=m_recv.at[i],
            device_id=(t * 2 + core, tp), device_id_type=MESH)
        c.start()
        metas.append(c)
    c = pltpu.make_async_copy(meta.at[rows_of(chip)], meta_in.at[pl.ds(OWN * 16, 16)], own_sem.at[CHUNKS])
    c.start()
    owns[CHUNKS] = c
    dispatch(1, FAR + NEAR)
    keep(1)
    pack(2)
    pack(3)
    c = pltpu.make_async_copy(out_w_h, out_w, local_sem.at[3])
    c.start()
    locals_.append(c)
    for c in edges:
        c.wait_recv()
    weights = []
    for i, (a, b) in enumerate(((gate_w, wg), (up_w, wu), (down_w, wd))):
        c = pltpu.make_async_remote_copy(
            src_ref=a, dst_ref=b.at[core], send_sem=w_send.at[i], recv_sem=w_recv.at[i],
            device_id=partner, device_id_type=MESH)
        c.start()
        own = pltpu.make_async_copy(a, b.at[core], w_own.at[i])
        own.start()
        weights.append((c, own))

    for k in range(2, CHUNKS):
        dispatch(k, FAR + NEAR)
        keep(k)

    def x_copy(src, dst, slot, k, to):
        return pltpu.make_async_remote_copy(
            src_ref=src, dst_ref=dst, send_sem=x_send.at[slot, k], recv_sem=x_recv.at[slot, k],
            device_id=(ep, to), device_id_type=MESH)

    pending = []

    def launch(c):
        c.start()
        pending.append(c)
        return c

    xs = {}
    returns, kept = {}, {}

    def compute(u):
        k, buf, base, count = UNITS[u]
        rows, top, low = pl.ds(base, count), pl.ds(base, count // 2), pl.ds(base + count // 2, count // 2)
        half = pl.ds(base // 2, count // 2)
        kinds = ((0,), (0, 1), (0, 1), (1,))[k]
        if len(kinds) == 2:
            lane = lax.broadcasted_iota(jnp.int32, (count, 128), 1)
            marks = jnp.where(lane == k, meta_in[rows, :].astype(jnp.float32), 0.0)
            is_even = jnp.sum(marks, axis=1, keepdims=True) > 0.5
        for e in kinds:
            g, v = None, None
            for q in range(4):
                x, deep = recv[k, q, rows, :], pl.ds(q * QUARTER, QUARTER)
                g_q = jnp.dot(x, wg[e, deep, :], preferred_element_type=jnp.float32)
                v_q = jnp.dot(x, wu[e, deep, :], preferred_element_type=jnp.float32)
                g, v = (g_q, v_q) if g is None else (g + g_q, v + v_q)
            h = g / (1.0 + jnp.exp(-g)) * v
            if len(kinds) == 2:
                h = jnp.where(is_even, h, 0.0) if e == 0 else jnp.where(is_even, 0.0, h)
            inner[e, rows, :] = h.astype(jnp.bfloat16)

        def quarter(q):
            def strip(n, carry):
                cols = pl.ds(pl.multiple_of(q * QUARTER + n * 512, 512), 512)
                total = None
                for e in kinds:
                    d = jnp.dot(inner[e, rows, :], wd[e, :, cols], preferred_element_type=jnp.float32)
                    total = d if total is None else total + d
                part[buf, q, rows, pl.ds(pl.multiple_of(n * 512, 512), 512)] = total.astype(jnp.bfloat16)
                return carry

            lax.fori_loop(0, 2, strip, 0)

        quarter(far)
        xs[u, 0] = launch(x_copy(part.at[buf, far, top], fwd_l.at[k, half], 0, u, right))
        xs[u, 1] = launch(x_copy(part.at[buf, far, low], fwd_r.at[k, half], 1, u, left))
        quarter(right)
        xs[u, 2] = launch(x_copy(part.at[buf, right, low], in_l.at[k, low], 2, u, right))
        quarter(left)
        xs[u, 3] = launch(x_copy(part.at[buf, left, top], in_r.at[k, top], 3, u, left))
        quarter(tp)

    def forward(u):
        k, buf, base, count = UNITS[u]
        top, low = pl.ds(base, count // 2), pl.ds(base + count // 2, count // 2)
        half = pl.ds(base // 2, count // 2)
        xs[u, 0].wait_recv()
        own = part[buf, right, top].astype(jnp.float32)
        fwd_l[k, half] = (fwd_l[k, half].astype(jnp.float32) + own).astype(jnp.bfloat16)
        xs[u, 4] = launch(x_copy(fwd_l.at[k, half], in_l.at[k, top], 4, u, right))
        xs[u, 1].wait_recv()
        own = part[buf, left, low].astype(jnp.float32)
        fwd_r[k, half] = (fwd_r[k, half].astype(jnp.float32) + own).astype(jnp.bfloat16)
        xs[u, 5] = launch(x_copy(fwd_r.at[k, half], in_r.at[k, low], 5, u, left))

    def finish(u):
        k, buf, base, count = UNITS[u]
        rows = pl.ds(base, count)
        for i in (2, 3, 4, 5):
            xs[u, i].wait_recv()
        in_l[k, rows] = (
            part[buf, tp, rows].astype(jnp.float32) + in_l[k, rows].astype(jnp.float32) + in_r[k, rows].astype(jnp.float32)
        ).astype(jnp.bfloat16)
        for i in hops_of(u):
            dz, dy = HOPS[i]
            t = chip_at(4 - dz, 4 - dy)
            returns[k, i] = launch(pltpu.make_async_remote_copy(
                src_ref=in_l.at[k, spot_of(i)], dst_ref=ret.at[k, rows_of(chip)],
                send_sem=r_send.at[k, i], recv_sem=r_recv.at[k, i],
                device_id=(t * 2 + core, tp), device_id_type=MESH))
        if base == 0:
            kept[k] = pltpu.make_async_copy(in_l.at[k, pl.ds(OWN * 16, 16)], ret.at[k, rows_of(chip)], r_own.at[k])
            kept[k].start()

    def combine(k):
        kept[k].wait()
        for i in range(len(HOPS)):
            returns[k, i].wait_recv()
        entry = k * ROWS + lax.broadcasted_iota(jnp.int32, (512, ROWS), 1)
        mix = jnp.where(entry == spot_cols[:, 0:1], weight_cols[:, 0:1], 0.0) + jnp.where(
            entry == spot_cols[:, 1:2], weight_cols[:, 1:2], 0.0
        )
        mix_hi = mix.astype(jnp.bfloat16)
        mix_lo = (mix - mix_hi.astype(jnp.float32)).astype(jnp.bfloat16)
        for n in range(2):
            f = pl.ds(n * 512, 512)
            total = jnp.dot(mix_hi, ret[k, :, f], preferred_element_type=jnp.float32)
            total = total + jnp.dot(mix_lo, ret[k, :, f], preferred_element_type=jnp.float32)
            if k == 0:
                acc[:, f] = total
            elif k < CHUNKS - 1:
                acc[:, f] += total
            else:
                out[:, f] = (acc[:, f] + total).astype(jnp.bfloat16)

    def head_rows(b, carry):
        rows = pl.ds(pl.multiple_of(b * 128, 128), 128)
        for h in range(4):
            vals = pl.ds(h * 256, 256)
            o = acc[rows, vals] + jnp.dot(
                scaled[rows, pl.ds(h * 128, 128)], incoming[pl.ds(h * 128, 128), :], preferred_element_type=jnp.float32
            )
            o = o - jnp.mean(o, axis=-1, keepdims=True)
            o = o * lax.rsqrt(jnp.mean(o * o, axis=-1, keepdims=True) + epsilon) * gain[0:1, vals]
            g = gate_rows[rows, vals].astype(jnp.float32)
            hidden[rows, vals] = (g / (1.0 + jnp.exp(-g)) * o).astype(jnp.bfloat16)
        return carry

    btop, blow = pl.ds(0, 64), pl.ds(64, 64)

    def block_part(n, q, lower, count):
        return mixed.at[n, q, pl.ds(lower, count)]

    def project(n):
        def strip(i, carry):
            cols = pl.ds(pl.multiple_of(n * QUARTER + i * 256, 256), 256)
            total = jnp.dot(hidden[...], out_w[:, cols], preferred_element_type=jnp.float32).astype(jnp.bfloat16)
            for q in range(4):
                mixed[n, q, :, pl.ds(pl.multiple_of(i * 256, 256), 256)] = total[
                    q * 128 : (q + 1) * 128
                ]
            return carry

        lax.fori_loop(0, 4, strip, 0)
        k = len(UNITS) + n
        xs[k, 0] = x_copy(block_part(n, far, 0, 64), b_fwd_l.at[n], 0, k, right)
        xs[k, 1] = x_copy(block_part(n, far, 64, 64), b_fwd_r.at[n], 1, k, left)
        xs[k, 2] = x_copy(block_part(n, right, 64, 64), b_in_l.at[n, blow], 2, k, right)
        xs[k, 3] = x_copy(block_part(n, left, 0, 64), b_in_r.at[n, btop], 3, k, left)
        for i in range(4):
            launch(xs[k, i])

    def pass_on(n):
        k = len(UNITS) + n
        for slot, buf, own, dst, to in (
            (0, b_fwd_l, block_part(n, right, 0, 64), b_in_l.at[n, btop], right),
            (1, b_fwd_r, block_part(n, left, 64, 64), b_in_r.at[n, blow], left),
        ):
            xs[k, slot].wait_recv()
            buf[n] = (buf[n].astype(jnp.float32) + own[...].astype(jnp.float32)).astype(jnp.bfloat16)
            xs[k, 4 + slot] = launch(x_copy(buf.at[n], dst, 4 + slot, k, to))

    def close(n):
        k = len(UNITS) + n
        for i in (2, 3, 4, 5):
            xs[k, i].wait_recv()
        mixer_out[:, pl.ds(n * QUARTER, QUARTER)] = (
            block_part(n, tp, 0, 128)[...].astype(jnp.float32)
            + b_in_l[n].astype(jnp.float32)
            + b_in_r[n].astype(jnp.float32)
        ).astype(jnp.bfloat16)

    for c in locals_[:2]:
        c.wait()
    lax.fori_loop(0, 4, head_rows, 0)
    locals_[2].wait()
    for n in range(4):
        project(n)
        if n > 0:
            pass_on(n - 1)
    pass_on(3)
    for c, own in weights:
        own.wait()
        c.wait_recv()
    owns[CHUNKS].wait()
    for c in metas:
        c.wait_recv()
    for u in range(len(UNITS)):
        k, _, base, _ = UNITS[u]
        for i in hops_of(u):
            sends[k, i].wait_recv()
        if base == 0:
            owns[k].wait()
        if u < 3:
            for i in range(len(HOPS)):
                sends[k, i].wait_send()
        if u == 3:
            for i in range(6):
                xs[0, i].wait_send()
        compute(u)
        if u > 0:
            finish(u - 1)
        forward(u)
        if u == 1:
            for n in range(4):
                close(n)
    combine(0)
    combine(1)
    finish(len(UNITS) - 1)
    combine(2)
    combine(CHUNKS - 1)
    for c, own in weights:
        c.wait_send()
    for c in metas + spreads + planes + edges:
        c.wait_send()
    for i in range(len(HOPS)):
        sends[CHUNKS - 1, i].wait_send()
    for c in pending:
        if all(c is not xs[0, i] for i in range(6)):
            c.wait_send()


HOPS = (
    (2, 0), (0, 2), (2, 1), (1, 2), (2, 3), (3, 2), (2, 2),
    (1, 0), (0, 1), (3, 0), (0, 3), (1, 1), (3, 3), (1, 3), (3, 1),
)
OWN = 7
ROW_HOPS = ((0, 1), (1, 0), (3, 0), (1, 1), (3, 1), (2, 0), (2, 1))
FAR, NEAR = tuple(range(7)), tuple(range(7, 15))
UNITS = ((0, 0, 0, 256), (1, 1, 0, 256), (2, 2, 0, 256), (3, 0, 0, 128), (3, 0, 128, 128))


def hops_of(u):
    base, count = UNITS[u][2:]
    return FAR + NEAR if count == ROWS else (FAR if base == 0 else NEAR)


def joint(
    rows, row_gain, route_ids, route_weight, gate_w, up_w, down_w, out_w, gate_rows, inside, scaled, state, ending, gain
):
    tokens, width = rows.shape
    experts = 32
    kinds = jnp.arange(experts, dtype=jnp.int32)
    one_hot = route_ids[:, :, None] == kinds[None, None, :]
    named = jnp.any(one_hot, axis=1).astype(jnp.bfloat16)
    steps = jnp.arange(tokens, dtype=jnp.int32)
    earlier = (steps[:, None] > steps[None, :]).astype(jnp.bfloat16)
    rank = jnp.dot(earlier, named, preferred_element_type=jnp.float32).astype(jnp.int32)
    slot = jnp.where(kinds % 2 == 0, rank, 63 - rank)
    place = (slot // 16) * ROWS + (kinds // 2) * 16 + slot % 16
    spot = jnp.sum(jnp.where(one_hot, place[:, None, :], 0), axis=2)
    spot_rows = jnp.pad(spot.T, ((0, 6), (0, 0)))
    spot_cols = jnp.pad(spot, ((0, 0), (0, 126)))
    weight_cols = jnp.pad(route_weight, ((0, 0), (0, 126)))
    even_count = jnp.sum(named.astype(jnp.float32), axis=0)[0::2].astype(jnp.int32)
    slots = jnp.arange(16, dtype=jnp.int32)[None, :, None] + 16 * jnp.arange(128, dtype=jnp.int32)[None, None, :]
    meta = (slots < even_count[:, None, None]).astype(jnp.bfloat16).reshape(256, 128)
    any_space, vmem = pl.BlockSpec(memory_space=pl.ANY), pl.BlockSpec(memory_space=pltpu.VMEM)
    bf = jnp.bfloat16
    dma = pltpu.SemaphoreType.DMA
    return pl.pallas_call(
        joint_kernel,
        out_shape=(
            jax.ShapeDtypeStruct((tokens, QUARTER), bf),
            jax.ShapeDtypeStruct((tokens // 4, width), bf),
        ),
        in_specs=[any_space] + [vmem] * 4 + [any_space] * 7 + [vmem] * 4,
        out_specs=(vmem, vmem),
        scratch_shapes=[
            pltpu.VMEM((CHUNKS, 4, ROWS, QUARTER), bf),
            pltpu.VMEM((256, 128), bf),
            pltpu.VMEM((2, width, 256), bf),
            pltpu.VMEM((2, width, 256), bf),
            pltpu.VMEM((2, 256, width), bf),
            pltpu.VMEM((2, ROWS, 256), bf),
            pltpu.VMEM((CHUNKS, 4, ROWS, QUARTER), bf),
            pltpu.VMEM((4, 4, 128, QUARTER), bf),
            pltpu.VMEM((CHUNKS, 128, QUARTER), bf),
            pltpu.VMEM((CHUNKS, 128, QUARTER), bf),
            pltpu.VMEM((CHUNKS, ROWS, QUARTER), bf),
            pltpu.VMEM((CHUNKS, ROWS, QUARTER), bf),
            pltpu.VMEM((CHUNKS, ROWS, QUARTER), bf),
            pltpu.VMEM((tokens, QUARTER), jnp.float32),
            pltpu.VMEM((1024, width), bf),
            pltpu.VMEM((tokens, 1024), bf),
            pltpu.VMEM((tokens, 1024), bf),
            pltpu.VMEM((8, 64, 256), bf),
            pltpu.VMEM((8, 8, 256), jnp.float32),
            pltpu.VMEM((8, 64, 256), jnp.float32),
            pltpu.VMEM((64, 256), bf),
            pltpu.VMEM((8, 256), jnp.float32),
            pltpu.VMEM((4, 64, 256), bf),
            pltpu.VMEM((4, 8, 256), jnp.float32),
            pltpu.VMEM((8, 64, 256), bf),
            pltpu.VMEM((512, 256), bf),
            pltpu.VMEM((4, 64, QUARTER), bf),
            pltpu.VMEM((4, 64, QUARTER), bf),
            pltpu.VMEM((4, 128, QUARTER), bf),
            pltpu.VMEM((4, 128, QUARTER), bf),
            dma((CHUNKS, 15)), dma((CHUNKS, 15)), dma((15,)), dma((15,)), dma((CHUNKS + 1,)),
            dma((3,)), dma((3,)), dma((3,)), dma((6, 9)), dma((6, 9)),
            dma((CHUNKS, 15)), dma((CHUNKS, 15)), dma((CHUNKS,)), dma((4,)), dma((27,)), dma((27,)),
        ],
        compiler_params=pltpu.CompilerParams(
            collective_id=0, has_side_effects=True, vmem_limit_bytes=67043328
        ),
    )(
        rows, row_gain.reshape(1, width), spot_rows, spot_cols, weight_cols, meta, gate_w[0], up_w[0], down_w[0],
        out_w, gate_rows, inside, scaled, state, ending, gain.reshape(1, 1024),
    )


def body(
    queries,
    key_rows,
    value_rows,
    gate_rows,
    log_decay,
    head_gain,
    out_weight,
    expert_input,
    input_gain,
    route_ids,
    route_weight,
    expert_gate,
    expert_up,
    expert_down,
):
    inside, scaled, state, ending = local_retention(queries, key_rows, value_rows, log_decay)
    expert_out, mixer_out = joint(
        expert_input, input_gain, route_ids, route_weight, expert_gate, expert_up, expert_down, out_weight, gate_rows,
        inside, scaled, state, ending, head_gain,
    )
    return (mixer_out, expert_out)


def solution(mesh):
    placed = (
        P("ep", "tp"),
        P("ep", "tp"),
        P("ep", "tp"),
        P("ep", "tp"),
        P("tp", "ep"),
        P("tp"),
        P("tp", None),
        P("ep", None),
        P(),
        P("ep", None),
        P("ep", None),
        P("ep", None, "tp"),
        P("ep", None, "tp"),
        P("ep", "tp", None),
    )
    return jax.shard_map(
        body,
        mesh=mesh,
        in_specs=placed,
        out_specs=(P(("ep", "tp"), None), P("ep", "tp")),
        check_vma=False,
    )
```

time: 194 us -> 173 us (0.89)
  Pallas kernels: 169 us -> 155 us
  matrix products: 7.43 us -> 0.29 us
  other arithmetic: 8.66 us -> 4.96 us
  local copies, waits for them, and re-layouts: 7.94 us -> 10.7 us
    pallas_call x1, Pallas kernels: 166 us -> 153 us  [joint(): pl.pallas_call(joint_kernel, out_shape=(jax.ShapeDtypeStruct((tokens, QUA...]
    dot_general x1 -> x0, matrix products: 7.13 us -> none  [joint(): jnp.dot(chosen.astype(jnp.bfloat16), normed, preferred_element_type=jnp.f...]
    reduce_sum x1 -> x0, other arithmetic: 3.09 us -> none  [body(): jnp.mean(widened * widened, axis=-1, keepdims=True) + epsilon]
    pad x0 -> x3, local copies, waits for them, and re-layouts: none -> 2.04 us  [the longest x1 0.72 us: joint(): spot_cols = jnp.pad(spot, ((0, 0), (0, 126)))]
    convert_element_type x1 -> x0, other arithmetic: 1.95 us -> none  [joint(): mix_lo = (mix - rounded).astype(jnp.bfloat16)]
    unnamed x28 -> x21, local copies, waits for them, and re-layouts: 6.61 us -> 6.5 us
where the time goes in v3:
time: 173 us; the launch traced here: 172 us
  Pallas kernels  155 us (90%)
  local copies, waits for them, and re-layouts  10.7 us (6%)
  other arithmetic  4.96 us (3%)
    pallas_call x1, Pallas kernels, joint(): pl.pallas_call(joint_kernel, out_shape=(jax.ShapeDtypeStruct((tokens, QUA...  153 us
    unnamed x21, local copies, waits for them, and re-layouts  6.5 us

profile of v3, /device:TPU:0, one launch (start us, length us, event | category | flops | bytes accessed | tf_op | source)
XLA Modules:
  0.0 171.9 jit_solution(15375929338296519036)
XLA Ops:
  0.6 0.0 copy-start.7
  0.7 0.7 reshape.81
  1.4 1.2 reduce-window.6
  2.6 0.2 slice_reduce_fusion
  2.8 0.2 reduce-window.9
  3.0 0.1 add_bitcast_fusion
  3.1 0.2 slice_reduce_fusion.1
  3.2 0.7 broadcast_in_dim.38.ending
  3.9 0.7 fusion
  4.6 0.1 convert_reduce_fusion
  4.7 0.1 slice.12
  4.9 0.1 lt.36
  4.9 0.1 lt.37
  5.0 0.3 fusion.5
  5.3 0.7 select_reduce_fusion
  6.0 0.6 pad.20.spot_rows
  6.7 0.7 fusion.1.meta
  7.4 0.1 copy.26
  7.5 0.0 copy-start.1
  7.5 0.0 copy-start.3
  7.5 0.0 copy-start.4
  7.6 0.7 pad.21.spot_cols
  8.3 0.1 copy.29
  8.5 0.0 copy-done.7
  8.5 0.1 copy.27
  8.6 0.7 pad.22.weight_cols
  9.3 1.0 fusion.2
  10.3 0.2 pad_maximum_fusion
  10.5 0.0 copy-done.1
  10.6 0.0 copy-done.3
  10.6 0.0 copy-done.4
  10.6 2.6 %shard_map.149 = (f32[512,1024]{1,0:T(8,128)S(1)}, bf16[512,512]{1,0:T(8,128)(2,1)S(1)}, bf16[512,256]{1,0:T(8,128)(2,1)S(1)}) custom-call(bf16[512,512]{1,0:T(8,128)(2,1)S(1)} %copy-done.3, bf16[512,512]{1,0:T(8,128)(2,1)S(1)} %copy-done.4, bf16[512,1024]{1,0:T(8,128)(2,1)S(1)} %copy-done.1, f32[512,128]{1,0:T(8,128)S(1)} %get-tuple-element.17.cosine, ...), custom_call_target="tpu_custom_call" | custom-call | tf_op jit(solution)/shard_map/pallas_call | solution.py:58
  13.2 0.0 copy-start
  13.2 1.3 copy-done
  14.5 0.0 copy-start.2
  14.5 0.8 copy-done.2
  15.3 0.0 copy-start.5
  15.3 0.7 copy-done.5
  16.0 152.5 %shard_map.150 = (bf16[512,1024]{1,0:T(8,128)(2,1)}, bf16[128,4096]{1,0:T(8,128)(2,1)}) custom-call(bf16[512,4096]{1,0:T(8,128)(2,1)} %rows_h.1, f32[1,4096]{1,0:T(1,128)} %bitcast.28, s32[8,512]{1,0:T(8,128)} %pad.20.spot_rows, s32[512,128]{1,0:T(8,128)} %pad.21.spot_cols, f32[512,128]{1,0:T(8,128)} %pad.22.weight_cols, bf16[256,128]{1,0:T(8,128)(2,1)} %fusion.1.meta, ...), custom_call_target="tpu_custom_call" | custom-call | tf_op jit(solution)/shard_map/pallas_call | solution.py:514
  168.5 0.0 copy-start.6
  168.6 2.4 %copy.37 = bf16[128,4096]{1,0:T(8,128)(2,1)} copy(bf16[128,4096]{1,0:T(8,128)(2,1)} %get-tuple-element.21) | data formatting | bytes 2097152
  170.9 0.0 copy-done.6
  170.9 1.0 copy.38
  (10 shorter events, 0.1 us)
Async XLA Ops:
  0.6 7.8 %copy-start.7 = (f32[512,2]{0,1:T(2,128)S(1)}, f32[512,2]{0,1:T(2,128)}, u32[]{:S(2)}) copy-start(f32[512,2]{0,1:T(2,128)} %param.24) | copy-start | bytes 12292
  7.5 3.0 %copy-start.1 = (bf16[512,1024]{1,0:T(8,128)(2,1)S(1)}, bf16[512,1024]{1,0:T(8,128)(2,1)}, u32[]{:S(2)}) copy-start(bf16[512,1024]{1,0:T(8,128)(2,1)} %value_rows.1) | copy-start | bytes 3145732
  7.5 3.0 %copy-start.3 = (bf16[512,512]{1,0:T(8,128)(2,1)S(1)}, bf16[512,512]{1,0:T(8,128)(2,1)}, u32[]{:S(2)}) copy-start(bf16[512,512]{1,0:T(8,128)(2,1)} %queries.1) | copy-start | bytes 1572868
  7.5 3.0 %copy-start.4 = (bf16[512,512]{1,0:T(8,128)(2,1)S(1)}, bf16[512,512]{1,0:T(8,128)(2,1)}, u32[]{:S(2)}) copy-start(bf16[512,512]{1,0:T(8,128)(2,1)} %key_rows.1) | copy-start | bytes 1572868
  13.2 1.4 copy-start
  14.5 0.8 copy-start.2
  15.3 0.7 copy-start.5
  168.5 2.4 %copy-start.6 = (bf16[512,1024]{1,0:T(8,128)(2,1)S(1)}, bf16[512,1024]{1,0:T(8,128)(2,1)}, u32[]{:S(2)}) copy-start(bf16[512,1024]{1,0:T(8,128)(2,1)} %get-tuple-element.22) | copy-start | bytes 3145732

commit v4 on v3

--- a/solution.py
+++ b/solution.py
@@ -9,67 +9,6 @@
 epsilon = 1e-06
 theta_base = 10000.0
 
-def local_kernel(queries, key_rows, value_rows, cosine, sine, run_cols, run_rows, inside, scaled, state, keys, mixed_q):
-    half = 64
-    for h in range(4):
-        cols, vals = pl.ds(h * 128, 128), pl.ds(h * 256, 256)
-        q = queries[:, cols].astype(jnp.float32)
-        k = key_rows[:, cols].astype(jnp.float32)
-        q = q * cosine[...] + pltpu.roll(q, half, 1) * sine[...]
-        k = (k * cosine[...] + pltpu.roll(k, half, 1) * sine[...]) * 128.0 ** (-0.5)
-        run = run_cols[:, h : h + 1]
-        ending = run_rows[h : h + 1, 511:512]
-        keys[...] = k.astype(jnp.bfloat16)
-        mixed_q[...] = q.astype(jnp.bfloat16)
-        scaled[:, cols] = (q * jnp.exp(run)).astype(jnp.bfloat16)
-        kept = (k * jnp.exp(ending - run)).astype(jnp.bfloat16)
-        state[pl.ds(h * 128, 128), :] = lax.dot_general(
-            kept, value_rows[:, vals], (((0,), (0,)), ((), ())), preferred_element_type=jnp.float32
-        ).astype(jnp.bfloat16)
-        for b in range(4):
-            rows, wide = pl.ds(b * 128, 128), (b + 1) * 128
-            scores = lax.dot_general(
-                mixed_q[rows, :], keys[pl.ds(0, wide), :], (((1,), (1,)), ((), ())),
-                preferred_element_type=jnp.float32,
-            )
-            spread = run_cols[rows, h : h + 1] - run_rows[h : h + 1, 0:wide]
-            here = b * 128 + lax.broadcasted_iota(jnp.int32, (128, wide), 0)
-            there = lax.broadcasted_iota(jnp.int32, (128, wide), 1)
-            table = jnp.exp(jnp.where(here >= there, spread, -jnp.inf))
-            inside[rows, vals] = jnp.dot(
-                (scores * table).astype(jnp.bfloat16), value_rows[pl.ds(0, wide), vals],
-                preferred_element_type=jnp.float32,
-            )
-
-
-def local_retention(queries, key_rows, value_rows, log_decay):
-    length = queries.shape[0]
-    half = 64
-    positions = (lax.axis_index("ep") * length + jnp.arange(length, dtype=jnp.int32)).astype(jnp.float32)
-    frequency = theta_base ** (-jnp.arange(half, dtype=jnp.float32) / half)
-    angles = positions[:, None] * frequency
-    cosine, sine = jnp.cos(angles), jnp.sin(angles)
-    cosine = jnp.concatenate([cosine, cosine], axis=1)
-    sine = jnp.concatenate([-sine, sine], axis=1)
-    running = jnp.cumsum(log_decay, axis=1)
-    run_rows = jnp.pad(running, ((0, 4), (0, 0)))
-    run_cols = jnp.pad(running.T, ((0, 0), (0, 124)))
-    ending = jnp.broadcast_to(run_rows[:, -1:], (8, 256))
-    inside, scaled, state = pl.pallas_call(
-        local_kernel,
-        out_shape=(
-            jax.ShapeDtypeStruct((length, 1024), jnp.float32),
-            jax.ShapeDtypeStruct((length, 512), jnp.bfloat16),
-            jax.ShapeDtypeStruct((512, 256), jnp.bfloat16),
-        ),
-        in_specs=[pl.BlockSpec(memory_space=pltpu.VMEM)] * 7,
-        out_specs=(pl.BlockSpec(memory_space=pltpu.VMEM),) * 3,
-        scratch_shapes=[pltpu.VMEM((length, 128), jnp.bfloat16), pltpu.VMEM((length, 128), jnp.bfloat16)],
-        compiler_params=pltpu.CompilerParams(vmem_limit_bytes=24 * 1024 * 1024),
-    )(queries, key_rows, value_rows, cosine, sine, run_cols, run_rows)
-    return inside, scaled, state, ending
-
-
 ROWS = 256
 CHUNKS = 4
 QUARTER = 1024
@@ -77,13 +16,14 @@
 
 
 def joint_kernel(
-    rows_h, row_gain, spot_rows, spot_cols, weight_cols, meta, gate_w, up_w, down_w, out_w_h, gate_rows_h, inside_h,
-    scaled, state, ending, gain,
+    rows_h, row_gain, ids_rows, ids_cols, weight_cols, gate_w, up_w, down_w, out_w_h, gate_rows_h, queries_h, keys_h,
+    values_h, cosine, sine, decays, gain,
     out, mixer_out,
     recv, meta_in, wg, wu, wd, inner, part, mixed, fwd_l, fwd_r, in_l, in_r, ret, acc, out_w, gate_rows,
     hidden, gathered, gathered_end, before, total_out, total_end, plane, plane_end, starts, incoming, b_fwd_l, b_fwd_r, b_in_l, b_in_r,
     d_send, d_recv, m_send, m_recv, own_sem, w_send, w_recv, w_own, x_send, x_recv, r_send, r_recv, r_own, local_sem,
-    s_send, s_recv,
+    s_send, s_recv, queries, key_rows, keys, turned, scaled, state, ending, decay_rows, run_cols, meta, spot_rows,
+    q_sem,
 ):
     ep, tp = lax.axis_index("ep"), lax.axis_index("tp")
     core, chip = ep % 2, ep // 2
@@ -112,12 +52,14 @@
     partner = (chip * 2 + 1 - core, tp)
     normed = out_w.at[pl.ds(0, 512)]
     rows_in = pltpu.make_async_copy(rows_h, normed, local_sem.at[0])
-    rows_in.start()
     locals_ = []
-    for i, (a, b) in enumerate(((inside_h, acc), (gate_rows_h, gate_rows))):
-        c = pltpu.make_async_copy(a, b, local_sem.at[1 + i])
+    for i, (a, b) in enumerate(((queries_h, queries), (keys_h, key_rows), (values_h, hidden))):
+        c = pltpu.make_async_copy(a, b, q_sem.at[i])
         c.start()
         locals_.append(c)
+    rows_in.start()
+    gate_in = pltpu.make_async_copy(gate_rows_h, gate_rows, local_sem.at[1])
+    gate_in.start()
 
     def state_copy(src, dst, i, to):
         c = pltpu.make_async_remote_copy(
@@ -125,17 +67,6 @@
             device_id=to, device_id_type=MESH)
         c.start()
         return c
-
-    rows_in.wait()
-
-    def norm_rows(b, carry):
-        rows = pl.ds(pl.multiple_of(b * 16, 16), 16)
-        v = out_w[rows, :].astype(jnp.float32)
-        scale = lax.rsqrt(jnp.mean(v * v, axis=-1, keepdims=True) + epsilon)
-        out_w[rows, :] = (v * scale * row_gain[...]).astype(jnp.bfloat16)
-        return carry
-
-    lax.fori_loop(0, 32, norm_rows, 0)
 
     def pack(k):
         entry = k * ROWS + lax.broadcasted_iota(jnp.int32, (ROWS, 512), 0)
@@ -166,6 +97,48 @@
         owns[k] = pltpu.make_async_copy(part.at[k, :, rows_of(chip)], recv.at[k, :, pl.ds(OWN * 16, 16)], own_sem.at[k])
         owns[k].start()
 
+    across = lax.broadcasted_iota(jnp.int32, (512, 512), 0)
+    along = lax.broadcasted_iota(jnp.int32, (512, 512), 1)
+    decay_rows[...] = jnp.zeros((8, 512), jnp.float32)
+    decay_rows[0:4, :] = decays[...]
+    each = decay_rows[...]
+    run_cols[:, 0:8] = lax.dot_general(
+        (across >= along).astype(jnp.float32), each, (((1,), (1,)), ((), ())),
+        precision=lax.Precision.HIGHEST, preferred_element_type=jnp.float32,
+    )
+    decay_rows[...] = jnp.dot(
+        each, (across <= along).astype(jnp.float32), precision=lax.Precision.HIGHEST, preferred_element_type=jnp.float32
+    )
+    ending[...] = jnp.broadcast_to(decay_rows[:, 511:512], (8, 256))
+    for c in locals_:
+        c.wait()
+    for h in range(4):
+        cols, vals = pl.ds(h * 128, 128), pl.ds(h * 256, 256)
+        q = queries[:, cols].astype(jnp.float32)
+        k = key_rows[:, cols].astype(jnp.float32)
+        q = q * cosine[...] + pltpu.roll(q, 64, 1) * sine[...]
+        k = (k * cosine[...] + pltpu.roll(k, 64, 1) * sine[...]) * 128.0 ** (-0.5)
+        run = run_cols[:, h : h + 1]
+        keys[...] = k.astype(jnp.bfloat16)
+        turned[...] = q.astype(jnp.bfloat16)
+        scaled[:, cols] = (q * jnp.exp(run)).astype(jnp.bfloat16)
+        held = (k * jnp.exp(decay_rows[h : h + 1, 511:512] - run)).astype(jnp.bfloat16)
+        state[pl.ds(h * 128, 128), :] = lax.dot_general(
+            held, hidden[:, vals], (((0,), (0,)), ((), ())), preferred_element_type=jnp.float32
+        ).astype(jnp.bfloat16)
+        for b in range(4):
+            rows, wide = pl.ds(b * 128, 128), (b + 1) * 128
+            scores = lax.dot_general(
+                turned[rows, :], keys[pl.ds(0, wide), :], (((1,), (1,)), ((), ())), preferred_element_type=jnp.float32
+            )
+            spread = run_cols[rows, h : h + 1] - decay_rows[h : h + 1, 0:wide]
+            here = b * 128 + lax.broadcasted_iota(jnp.int32, (128, wide), 0)
+            there = lax.broadcasted_iota(jnp.int32, (128, wide), 1)
+            table = jnp.exp(jnp.where(here >= there, spread, -jnp.inf))
+            acc[rows, vals] = jnp.dot(
+                (scores * table).astype(jnp.bfloat16), hidden[pl.ds(0, wide), vals], preferred_element_type=jnp.float32
+            )
+
     pl.semaphore_wait(barrier, len(HOPS) + 6)
     place = y * 2 + core
     head = place // 2
@@ -182,7 +155,41 @@
         to = ((z * 4 + py) * 2 + pc, tp)
         spreads.append(state_copy(state.at[slice_of(py * 2 + pc)], gathered.at[place], i, to))
         spreads.append(state_copy(ending, gathered_end.at[place], 7 + i, to))
-    pack(0)
+
+    def places(rank, kinds):
+        slot = jnp.where(kinds % 2 == 0, rank, 63 - rank)
+        return (slot >> 4) * ROWS + (kinds >> 1) * 16 + (slot & 15)
+
+    kinds = lax.broadcasted_iota(jnp.int32, (32, 512), 0)
+    first, second = kinds == ids_rows[0:1, :], kinds == ids_rows[1:2, :]
+    named = jnp.where(first | second, 1.0, 0.0).astype(jnp.bfloat16)
+    rank = jnp.dot(named, jnp.where(across < along, 1.0, 0.0).astype(jnp.bfloat16), preferred_element_type=jnp.float32)
+    spots = places(rank.astype(jnp.int32), kinds)
+    spot_rows[0:1, :] = jnp.sum(jnp.where(first, spots, 0), axis=0, keepdims=True)
+    spot_rows[1:2, :] = jnp.sum(jnp.where(second, spots, 0), axis=0, keepdims=True)
+    owner = lax.broadcasted_iota(jnp.int32, (256, 32), 0) >> 4
+    evens = jnp.where(lax.broadcasted_iota(jnp.int32, (256, 32), 1) == 2 * owner, 1.0, 0.0).astype(jnp.bfloat16)
+    count = jnp.sum(jnp.dot(evens, named, preferred_element_type=jnp.float32), axis=1, keepdims=True)
+    level = (lax.broadcasted_iota(jnp.int32, (256, 128), 0) & 15) + 16 * lax.broadcasted_iota(jnp.int32, (256, 128), 1)
+    meta[...] = jnp.where(level.astype(jnp.float32) < count, 1.0, 0.0).astype(jnp.bfloat16)
+    kinds = lax.broadcasted_iota(jnp.int32, (512, 128), 1)
+    first, second = kinds == ids_cols[:, 0:1], kinds == ids_cols[:, 1:2]
+    named = jnp.where(first | second, 1.0, 0.0).astype(jnp.bfloat16)
+    rank = jnp.dot(jnp.where(across > along, 1.0, 0.0).astype(jnp.bfloat16), named, preferred_element_type=jnp.float32)
+    spots = places(rank.astype(jnp.int32), kinds)
+    run_cols[:, 8:9] = jnp.sum(jnp.where(first, spots, 0).astype(jnp.float32), axis=1, keepdims=True)
+    run_cols[:, 9:10] = jnp.sum(jnp.where(second, spots, 0).astype(jnp.float32), axis=1, keepdims=True)
+    rows_in.wait()
+
+    def norm_rows(b, carry):
+        rows = pl.ds(pl.multiple_of(b * 16, 16), 16)
+        v = out_w[rows, :].astype(jnp.float32)
+        scale = lax.rsqrt(jnp.mean(v * v, axis=-1, keepdims=True) + epsilon)
+        out_w[rows, :] = (v * scale * row_gain[...]).astype(jnp.bfloat16)
+        return carry
+
+    lax.fori_loop(0, 32, norm_rows, 0)
+
     gathered[place] = state[slice_of(place), :]
     gathered_end[place] = ending[...]
     for c in spreads:
@@ -202,7 +209,7 @@
         to = ((((z + d) % 4) * 4 + y) * 2 + core, tp)
         planes.append(state_copy(total_out, plane.at[z], 12 + 2 * d, to))
         planes.append(state_copy(total_end, plane_end.at[z], 13 + 2 * d, to))
-    pack(1)
+    pack(0)
     plane[z] = carried.astype(jnp.bfloat16)
     plane_end[z] = jnp.broadcast_to(reach, (8, 256))
     for c in planes:
@@ -233,13 +240,13 @@
     c = pltpu.make_async_copy(meta.at[rows_of(chip)], meta_in.at[pl.ds(OWN * 16, 16)], own_sem.at[CHUNKS])
     c.start()
     owns[CHUNKS] = c
+    pack(1)
     dispatch(1, FAR + NEAR)
     keep(1)
     pack(2)
     pack(3)
-    c = pltpu.make_async_copy(out_w_h, out_w, local_sem.at[3])
-    c.start()
-    locals_.append(c)
+    out_w_in = pltpu.make_async_copy(out_w_h, out_w, local_sem.at[2])
+    out_w_in.start()
     for c in edges:
         c.wait_recv()
     weights = []
@@ -349,9 +356,9 @@
         kept[k].wait()
         for i in range(len(HOPS)):
             returns[k, i].wait_recv()
-        entry = k * ROWS + lax.broadcasted_iota(jnp.int32, (512, ROWS), 1)
-        mix = jnp.where(entry == spot_cols[:, 0:1], weight_cols[:, 0:1], 0.0) + jnp.where(
-            entry == spot_cols[:, 1:2], weight_cols[:, 1:2], 0.0
+        entry = (k * ROWS + lax.broadcasted_iota(jnp.int32, (512, ROWS), 1)).astype(jnp.float32)
+        mix = jnp.where(entry == run_cols[:, 8:9], weight_cols[:, 0:1], 0.0) + jnp.where(
+            entry == run_cols[:, 9:10], weight_cols[:, 1:2], 0.0
         )
         mix_hi = mix.astype(jnp.bfloat16)
         mix_lo = (mix - mix_hi.astype(jnp.float32)).astype(jnp.bfloat16)
@@ -423,10 +430,9 @@
             + b_in_r[n].astype(jnp.float32)
         ).astype(jnp.bfloat16)
 
-    for c in locals_[:2]:
-        c.wait()
+    gate_in.wait()
     lax.fori_loop(0, 4, head_rows, 0)
-    locals_[2].wait()
+    out_w_in.wait()
     for n in range(4):
         project(n)
         if n > 0:
@@ -489,25 +495,16 @@
 
 
 def joint(
-    rows, row_gain, route_ids, route_weight, gate_w, up_w, down_w, out_w, gate_rows, inside, scaled, state, ending, gain
+    queries, key_rows, value_rows, gate_rows, log_decay, gain, out_w, rows, row_gain, route_ids, route_weight,
+    gate_w, up_w, down_w,
 ):
     tokens, width = rows.shape
-    experts = 32
-    kinds = jnp.arange(experts, dtype=jnp.int32)
-    one_hot = route_ids[:, :, None] == kinds[None, None, :]
-    named = jnp.any(one_hot, axis=1).astype(jnp.bfloat16)
-    steps = jnp.arange(tokens, dtype=jnp.int32)
-    earlier = (steps[:, None] > steps[None, :]).astype(jnp.bfloat16)
-    rank = jnp.dot(earlier, named, preferred_element_type=jnp.float32).astype(jnp.int32)
-    slot = jnp.where(kinds % 2 == 0, rank, 63 - rank)
-    place = (slot // 16) * ROWS + (kinds // 2) * 16 + slot % 16
-    spot = jnp.sum(jnp.where(one_hot, place[:, None, :], 0), axis=2)
-    spot_rows = jnp.pad(spot.T, ((0, 6), (0, 0)))
-    spot_cols = jnp.pad(spot, ((0, 0), (0, 126)))
-    weight_cols = jnp.pad(route_weight, ((0, 0), (0, 126)))
-    even_count = jnp.sum(named.astype(jnp.float32), axis=0)[0::2].astype(jnp.int32)
-    slots = jnp.arange(16, dtype=jnp.int32)[None, :, None] + 16 * jnp.arange(128, dtype=jnp.int32)[None, None, :]
-    meta = (slots < even_count[:, None, None]).astype(jnp.bfloat16).reshape(256, 128)
+    half = 64
+    positions = (lax.axis_index("ep") * tokens + jnp.arange(tokens, dtype=jnp.int32)).astype(jnp.float32)
+    frequency = theta_base ** (-(jnp.arange(2 * half, dtype=jnp.int32) % half).astype(jnp.float32) / half)
+    angles = positions[:, None] * frequency
+    cosine = jnp.cos(angles)
+    sine = jnp.where(jnp.arange(2 * half) < half, -1.0, 1.0) * jnp.sin(angles)
     any_space, vmem = pl.BlockSpec(memory_space=pl.ANY), pl.BlockSpec(memory_space=pltpu.VMEM)
     bf = jnp.bfloat16
     dma = pltpu.SemaphoreType.DMA
@@ -517,7 +514,7 @@
             jax.ShapeDtypeStruct((tokens, QUARTER), bf),
             jax.ShapeDtypeStruct((tokens // 4, width), bf),
         ),
-        in_specs=[any_space] + [vmem] * 4 + [any_space] * 7 + [vmem] * 4,
+        in_specs=[any_space] + [vmem] * 4 + [any_space] * 8 + [vmem] * 4,
         out_specs=(vmem, vmem),
         scratch_shapes=[
             pltpu.VMEM((CHUNKS, 4, ROWS, QUARTER), bf),
@@ -553,13 +550,19 @@
             dma((CHUNKS, 15)), dma((CHUNKS, 15)), dma((15,)), dma((15,)), dma((CHUNKS + 1,)),
             dma((3,)), dma((3,)), dma((3,)), dma((6, 9)), dma((6, 9)),
             dma((CHUNKS, 15)), dma((CHUNKS, 15)), dma((CHUNKS,)), dma((4,)), dma((27,)), dma((27,)),
+            pltpu.VMEM((tokens, 512), bf), pltpu.VMEM((tokens, 512), bf),
+            pltpu.VMEM((tokens, 128), bf), pltpu.VMEM((tokens, 128), bf),
+            pltpu.VMEM((tokens, 512), bf), pltpu.VMEM((512, 256), bf), pltpu.VMEM((8, 256), jnp.float32),
+            pltpu.VMEM((8, tokens), jnp.float32), pltpu.VMEM((tokens, 128), jnp.float32), pltpu.VMEM((256, 128), bf),
+            pltpu.VMEM((8, tokens), jnp.int32), dma((3,)),
+
         ],
         compiler_params=pltpu.CompilerParams(
             collective_id=0, has_side_effects=True, vmem_limit_bytes=67043328
         ),
     )(
-        rows, row_gain.reshape(1, width), spot_rows, spot_cols, weight_cols, meta, gate_w[0], up_w[0], down_w[0],
-        out_w, gate_rows, inside, scaled, state, ending, gain.reshape(1, 1024),
+        rows, row_gain.reshape(1, width), route_ids.T, route_ids, route_weight, gate_w[0], up_w[0], down_w[0],
+        out_w, gate_rows, queries, key_rows, value_rows, cosine, sine, log_decay, gain.reshape(1, 1024),
     )
 
 
@@ -579,10 +582,9 @@
     expert_up,
     expert_down,
 ):
-    inside, scaled, state, ending = local_retention(queries, key_rows, value_rows, log_decay)
     expert_out, mixer_out = joint(
-        expert_input, input_gain, route_ids, route_weight, expert_gate, expert_up, expert_down, out_weight, gate_rows,
-        inside, scaled, state, ending, head_gain,
+        queries, key_rows, value_rows, gate_rows, log_decay, head_gain, out_weight, expert_input, input_gain,
+        route_ids, route_weight, expert_gate, expert_up, expert_down,
     )
     return (mixer_out, expert_out)
 

time: 173 us -> 161 us (0.931)
  local copies, waits for them, and re-layouts: 10.7 us -> 6.43 us
  other arithmetic: 4.96 us -> 1.81 us
  Pallas kernels: 155 us -> 152 us
    pallas_call x1 -> x0, Pallas kernels: 2.59 us -> none  [local_retention(): pl.pallas_call(local_kernel, out_shape=(jax.ShapeDtypeStruct((length, 102...]
    pad x5 -> x0, local copies, waits for them, and re-layouts: 2.07 us -> none  [the longest x1 0.72 us: joint(): spot_cols = jnp.pad(spot, ((0, 0), (0, 126)))]
    mul x2 -> x1, other arithmetic: 0.01 us -> 1.79 us  [joint(): sine = jnp.where(jnp.arange(2 * half) < half, -1.0, 1.0) * jnp.sin(angles)]
    unnamed x21 -> x6, local copies, waits for them, and re-layouts: 6.5 us -> 6.43 us
where the time goes in v4:
time: 161 us
  Pallas kernels  152 us (94%)
  local copies, waits for them, and re-layouts  6.43 us (4%)
  other arithmetic  1.81 us (1%)
    pallas_call x1, Pallas kernels, joint(): pl.pallas_call(joint_kernel, out_shape=(jax.ShapeDtypeStruct((tokens, QUA...  152 us
    unnamed x6, local copies, waits for them, and re-layouts  6.43 us

profile of v4, /device:TPU:0, one launch (start us, length us, event | category | flops | bytes accessed | tf_op | source)
XLA Modules:
  0.0 161.2 jit_solution(841090553341743019)
XLA Ops:
  0.7 1.5 copy.17.weight_cols
  2.2 1.5 copy.16.ids_cols
  3.7 1.8 %fusion = (f32[512,128]{1,0:T(8,128)}, f32[512,128]{1,0:T(8,128)}) fusion(f32[128]{0:T(128)S(1)} %get-tuple-element.8, f32[128]{0:T(128)S(1)} %get-tuple-element.9, f32[512]{0:T(512)S(1)} %add_convert_fusion), kind=kLoop, calls=%fused_computation.2 | loop fusion | flops 131072 | bytes 527360 | tf_op jit(solution)/shard_map/mul | solution.py:507
  5.5 152.3 %shard_map.149 = (bf16[512,1024]{1,0:T(8,128)(2,1)}, bf16[128,4096]{1,0:T(8,128)(2,1)}) custom-call(bf16[512,4096]{1,0:T(8,128)(2,1)} %rows_h.1, f32[1,4096]{1,0:T(1,128)} %bitcast.9, s32[2,512]{1,0:T(2,128)} %bitcast.10, s32[512,2]{1,0:T(8,128)} %copy.16.ids_cols, f32[512,2]{1,0:T(8,128)} %copy.17.weight_cols, bf16[4096,256]{1,0:T(8,128)(2,1)} %bitcast.6, ...), custom_call_target="tpu_custom_call" | custom-call | tf_op jit(solution)/shard_map/pallas_call | solution.py:511
  157.8 0.0 copy-start
  157.9 2.4 %copy.20 = bf16[128,4096]{1,0:T(8,128)(2,1)} copy(bf16[128,4096]{1,0:T(8,128)(2,1)} %get-tuple-element.12) | data formatting | bytes 2097152
  160.2 0.0 copy-done
  160.2 1.0 copy.21
  (2 shorter events, 0.0 us)
Async XLA Ops:
  157.8 2.4 %copy-start = (bf16[512,1024]{1,0:T(8,128)(2,1)S(1)}, bf16[512,1024]{1,0:T(8,128)(2,1)}, u32[]{:S(2)}) copy-start(bf16[512,1024]{1,0:T(8,128)(2,1)} %get-tuple-element.13) | copy-start | bytes 3145732

commit v5 on v4

--- a/solution.py
+++ b/solution.py
@@ -16,7 +16,7 @@
 
 
 def joint_kernel(
-    rows_h, row_gain, ids_rows, ids_cols, weight_cols, gate_w, up_w, down_w, out_w_h, gate_rows_h, queries_h, keys_h,
+    rows_h, row_gain, ids_rows, weight_rows, gate_w, up_w, down_w, out_w_h, gate_rows_h, queries_h, keys_h,
     values_h, cosine, sine, decays, gain,
     out, mixer_out,
     recv, meta_in, wg, wu, wd, inner, part, mixed, fwd_l, fwd_r, in_l, in_r, ret, acc, out_w, gate_rows,
@@ -99,11 +99,16 @@
 
     across = lax.broadcasted_iota(jnp.int32, (512, 512), 0)
     along = lax.broadcasted_iota(jnp.int32, (512, 512), 1)
-    decay_rows[...] = jnp.zeros((8, 512), jnp.float32)
     decay_rows[0:4, :] = decays[...]
+    decay_rows[4:6, :] = weight_rows[...]
+    decay_rows[6:8, :] = ids_rows[...].astype(jnp.float32)
     each = decay_rows[...]
     run_cols[:, 0:8] = lax.dot_general(
         (across >= along).astype(jnp.float32), each, (((1,), (1,)), ((), ())),
+        precision=lax.Precision.HIGHEST, preferred_element_type=jnp.float32,
+    )
+    run_cols[:, 16:24] = lax.dot_general(
+        (across == along).astype(jnp.float32), each, (((1,), (1,)), ((), ())),
         precision=lax.Precision.HIGHEST, preferred_element_type=jnp.float32,
     )
     decay_rows[...] = jnp.dot(
@@ -173,7 +178,7 @@
     level = (lax.broadcasted_iota(jnp.int32, (256, 128), 0) & 15) + 16 * lax.broadcasted_iota(jnp.int32, (256, 128), 1)
     meta[...] = jnp.where(level.astype(jnp.float32) < count, 1.0, 0.0).astype(jnp.bfloat16)
     kinds = lax.broadcasted_iota(jnp.int32, (512, 128), 1)
-    first, second = kinds == ids_cols[:, 0:1], kinds == ids_cols[:, 1:2]
+    first, second = kinds == run_cols[:, 22:23].astype(jnp.int32), kinds == run_cols[:, 23:24].astype(jnp.int32)
     named = jnp.where(first | second, 1.0, 0.0).astype(jnp.bfloat16)
     rank = jnp.dot(jnp.where(across > along, 1.0, 0.0).astype(jnp.bfloat16), named, preferred_element_type=jnp.float32)
     spots = places(rank.astype(jnp.int32), kinds)
@@ -210,6 +215,7 @@
         planes.append(state_copy(total_out, plane.at[z], 12 + 2 * d, to))
         planes.append(state_copy(total_end, plane_end.at[z], 13 + 2 * d, to))
     pack(0)
+    pack(1)
     plane[z] = carried.astype(jnp.bfloat16)
     plane_end[z] = jnp.broadcast_to(reach, (8, 256))
     for c in planes:
@@ -240,7 +246,6 @@
     c = pltpu.make_async_copy(meta.at[rows_of(chip)], meta_in.at[pl.ds(OWN * 16, 16)], own_sem.at[CHUNKS])
     c.start()
     owns[CHUNKS] = c
-    pack(1)
     dispatch(1, FAR + NEAR)
     keep(1)
     pack(2)
@@ -357,8 +362,8 @@
         for i in range(len(HOPS)):
             returns[k, i].wait_recv()
         entry = (k * ROWS + lax.broadcasted_iota(jnp.int32, (512, ROWS), 1)).astype(jnp.float32)
-        mix = jnp.where(entry == run_cols[:, 8:9], weight_cols[:, 0:1], 0.0) + jnp.where(
-            entry == run_cols[:, 9:10], weight_cols[:, 1:2], 0.0
+        mix = jnp.where(entry == run_cols[:, 8:9], run_cols[:, 20:21], 0.0) + jnp.where(
+            entry == run_cols[:, 9:10], run_cols[:, 21:22], 0.0
         )
         mix_hi = mix.astype(jnp.bfloat16)
         mix_lo = (mix - mix_hi.astype(jnp.float32)).astype(jnp.bfloat16)
@@ -514,7 +519,7 @@
             jax.ShapeDtypeStruct((tokens, QUARTER), bf),
             jax.ShapeDtypeStruct((tokens // 4, width), bf),
         ),
-        in_specs=[any_space] + [vmem] * 4 + [any_space] * 8 + [vmem] * 4,
+        in_specs=[any_space] + [vmem] * 3 + [any_space] * 8 + [vmem] * 4,
         out_specs=(vmem, vmem),
         scratch_shapes=[
             pltpu.VMEM((CHUNKS, 4, ROWS, QUARTER), bf),
@@ -561,7 +566,7 @@
             collective_id=0, has_side_effects=True, vmem_limit_bytes=67043328
         ),
     )(
-        rows, row_gain.reshape(1, width), route_ids.T, route_ids, route_weight, gate_w[0], up_w[0], down_w[0],
+        rows, row_gain.reshape(1, width), route_ids.T, route_weight.T, gate_w[0], up_w[0], down_w[0],
         out_w, gate_rows, queries, key_rows, value_rows, cosine, sine, log_decay, gain.reshape(1, 1024),
     )
 

time: 161 us -> 163 us (1.012); the launches traced: 161 us -> 161 us
  local copies, waits for them, and re-layouts: 6.43 us -> 3.35 us
  Pallas kernels: 152 us -> 155 us
    unnamed x6 -> x4, local copies, waits for them, and re-layouts: 6.43 us -> 3.35 us
    pallas_call x1, Pallas kernels: 152 us -> 155 us  [joint(): pl.pallas_call(joint_kernel, out_shape=(jax.ShapeDtypeStruct((tokens, QUA...]
where the time goes in v5:
time: 163 us; the launch traced here: 161 us
  Pallas kernels  155 us (95%)
  local copies, waits for them, and re-layouts  3.35 us (2%)
  other arithmetic  1.84 us (1%)
    pallas_call x1, Pallas kernels, joint(): pl.pallas_call(joint_kernel, out_shape=(jax.ShapeDtypeStruct((tokens, QUA...  155 us
    unnamed x4, local copies, waits for them, and re-layouts  3.35 us

profile of v5, /device:TPU:0, one launch (start us, length us, event | category | flops | bytes accessed | tf_op | source)
XLA Modules:
  0.0 160.6 jit_solution(17958064020420630393)
XLA Ops:
  0.7 1.8 %fusion = (f32[512,128]{1,0:T(8,128)}, f32[512,128]{1,0:T(8,128)}) fusion(f32[128]{0:T(128)S(1)} %get-tuple-element.8, f32[128]{0:T(128)S(1)} %get-tuple-element.9, f32[512]{0:T(512)S(1)} %add_convert_fusion), kind=kLoop, calls=%fused_computation.2 | loop fusion | flops 131072 | bytes 527360 | tf_op jit(solution)/shard_map/mul | solution.py:512
  2.5 154.7 %shard_map.149 = (bf16[512,1024]{1,0:T(8,128)(2,1)}, bf16[128,4096]{1,0:T(8,128)(2,1)}) custom-call(bf16[512,4096]{1,0:T(8,128)(2,1)} %rows_h.1, f32[1,4096]{1,0:T(1,128)} %bitcast.10, s32[2,512]{1,0:T(2,128)} %bitcast.11, f32[2,512]{1,0:T(2,128)} %bitcast.12, bf16[4096,256]{1,0:T(8,128)(2,1)} %bitcast.7, bf16[4096,256]{1,0:T(8,128)(2,1)} %bitcast.8, ...), custom_call_target="tpu_custom_call" | custom-call | tf_op jit(solution)/shard_map/pallas_call | solution.py:516
  157.2 0.0 copy-start
  157.2 2.4 %copy.18 = bf16[128,4096]{1,0:T(8,128)(2,1)} copy(bf16[128,4096]{1,0:T(8,128)(2,1)} %get-tuple-element.12) | data formatting | bytes 2097152
  159.6 0.0 copy-done
  159.6 1.0 copy.19
  (2 shorter events, 0.0 us)
Async XLA Ops:
  157.2 2.4 %copy-start = (bf16[512,1024]{1,0:T(8,128)(2,1)S(1)}, bf16[512,1024]{1,0:T(8,128)(2,1)}, u32[]{:S(2)}) copy-start(bf16[512,1024]{1,0:T(8,128)(2,1)} %get-tuple-element.13) | copy-start | bytes 3145732
